TPU v7x, 256 devices: a whole 4x4x8 slice. The times are simulated.
256 devices in a mesh: ep: 64 (over z, y, core), tp: 4 (over x).
Axes of the slice: x: 4, y: 4, z: 8, core: 2. Of those that a mesh axis runs over, the one named last changes fastest.
Arguments:
- queries: bfloat16 [32768, 512], P('ep', 'tp'), may hold values from -6 to 6
- key_rows: bfloat16 [32768, 512], P('ep', 'tp'), may hold values from -6 to 6
- value_rows: bfloat16 [32768, 1024], P('ep', 'tp'), may hold values from -6 to 6
- forget_gate_input: bfloat16 [32768, 512], P('ep', 'tp'), may hold values from -6 to 6
- channel_decay_rate: float32 [512], P('tp'), may hold values from 0 to 1, as said below
- position_decay_factor: float32 [32768], P('ep'), may hold values from 0 to 3, as said below
- extra_log_decay: float32 [32768, 8], P('ep', 'tp'), may hold values from -1 to 0, as said below
- head_norm_gain: float32 [8, 128], P('tp'), may hold values from 0.1 to 1.9
- output_projection_weight: bfloat16 [1024, 2048], P('tp'), may hold values from -0.1875 to 0.1875
- expert_input_rows: bfloat16 [16384, 2048], P('ep'), may hold values from -6 to 6
- expert_norm_gain: float32 [2048], replicated, may hold values from 0.1 to 1.9
- routes: int32 [16384, 2], P('ep'), may hold values from 0 to 63, all different within a row; in each aligned block of 256 rows (0 to 255, 256 to 511, ...) at most 16 rows name the same one
- chosen_expert_weights: float32 [16384, 2], P('ep'), may hold values from 0.2 to 1
- expert_gate_weight: bfloat16 [64, 2048, 3072], P('ep', None, 'tp'), may hold values from -0.125 to 0.125
- expert_up_weight: bfloat16 [64, 2048, 3072], P('ep', None, 'tp'), may hold values from -0.125 to 0.125
- expert_down_weight: bfloat16 [64, 3072, 2048], P('ep', 'tp'), may hold values from -0.109375 to 0.109375
Outputs:
- token_mixer_output: bfloat16 [32768, 2048], P(('ep', 'tp'))
- moe_out: bfloat16 [16384, 2048], P('ep', 'tp')
Inputs may be any that keep to these rules, and one draw needn't show every extreme that they name: `routes`: within the rows of one device no expert is named by more than 16 of the choices, a bound that some block reaches; the 2 experts of a token differ. `channel_decay_rate`: Positive. `position_decay_factor`: Positive. `extra_log_decay`: zero or negative.
All inputs are finite; a program needn't handle non-finite values.
Results may differ from a plain program's by a relative error of at most 0.019.
Values may be sent and summed in bfloat16 or wider, within the bound.
A program may use at most 128 MiB of HBM per device.

v0:
```python
import jax
import jax.numpy as jnp
from jax import lax
from jax.sharding import Mesh
from jax.sharding import PartitionSpec as P

KEY_CHANNELS = 64
VALUE_DIM = 128
SPAN = 64
EP = ("ep_0", "ep_1", "ep_2")
EP_TP = ("ep_0", "ep_1", "ep_2", "tp")


highest_precision = lax.Precision.HIGHEST
norm_eps = 1e-06


def nothing_yet(value, identity):
    return jax.tree.map(
        lambda a, e: jnp.broadcast_to(jnp.asarray(e, a.dtype), a.shape), value, identity
    )


def gathered_once(value, axis):
    leaves = jax.tree.leaves(value)
    order = sorted(range(len(leaves)), key=lambda k: -leaves[k].size)
    width = (1, *leaves[order[0]].shape)[-1]
    lines = [
        jnp.pad(leaves[k].reshape(-1), (0, -leaves[k].size % width)).reshape(-1, width)
        for k in order
    ]
    both, at, found = (lax.all_gather(jnp.concatenate(lines), axis), 0, {})
    for k, line in zip(order, lines):
        section = both[:, at : at + len(line)].reshape(len(both), -1)
        found[k] = section[:, : leaves[k].size].reshape(-1, *leaves[k].shape)
        at += len(line)
    numbers = iter(range(len(leaves)))
    return jax.tree.map(lambda _: found[next(numbers)], value)


def carried_in(value, axes, combine, identity):
    before = start = nothing_yet(value, identity)
    total = value
    for axis in reversed(axes):
        peers, index = (lax.axis_size(axis), lax.axis_index(axis))
        pieces = gathered_once(
            jax.tree.map(lambda part, kind: part.astype(kind), total, (jnp.bfloat16, jnp.bfloat16)),
            axis,
        )
        inside, total = (start, start)
        for k in range(peers):
            passed = k < index
            total = combine(
                total, jax.tree.map(lambda part, own: part[k].astype(own.dtype), pieces, value)
            )
            inside = jax.tree.map(lambda new, old: jnp.where(passed, new, old), total, inside)
        before = combine(inside, before)
    return before


def in_blocks(value, dim, peers):
    shape = value.shape
    tiles = value.reshape(*shape[:dim], peers, shape[dim] // peers, *shape[dim + 1 :])
    return jnp.moveaxis(tiles, dim, 0)


def sent_and_summed(value, axis, dim):
    tiles = in_blocks(value, dim, lax.axis_size(axis))
    arrived = lax.all_to_all(tiles, axis, split_axis=0, concat_axis=0, tiled=True)
    return arrived.astype(jnp.float32).sum(axis=0)


def gla_blocks(query_single, key_float, value_float, decay_logarithm, span_rows):
    length, head_count, key_width = query_single.shape
    value_width = value_float.shape[-1]
    block_count = length // span_rows

    def blocked(tensor):
        return tensor.reshape(block_count, span_rows, head_count, tensor.shape[-1])

    causal = (jnp.arange(span_rows)[:, None] >= jnp.arange(span_rows)[None, :])[:, :, None, None]

    def advance(carried_state, pieces):
        block_queries, block_keys, block_values, gate_block = pieces
        cumulative_decay = jnp.cumsum(gate_block, axis=0)
        log_gaps = cumulative_decay[:, None] - cumulative_decay[None, :]
        decays = jnp.exp(jnp.where(causal, log_gaps, -jnp.inf))
        scores = jnp.sum(block_queries[:, None] * block_keys[None, :] * decays, axis=-1)
        final_output = jnp.einsum("ijh,jhv->ihv", scores, block_values, precision=highest_precision)
        final_output = final_output + jnp.einsum(
            "nwt,wto->nwo",
            block_queries * jnp.exp(cumulative_decay),
            carried_state,
            precision=highest_precision,
        )
        final_log_decay = cumulative_decay[-1]
        carried_state = jnp.exp(final_log_decay)[:, :, None] * carried_state + jnp.einsum(
            "ygc,yga->gca",
            block_keys * jnp.exp(final_log_decay[None] - cumulative_decay),
            block_values,
            precision=highest_precision,
        )
        return (carried_state, final_output)

    start_state = jnp.zeros((head_count, key_width, value_width), jnp.float32)
    carried_state, outputs = lax.scan(
        advance,
        start_state,
        (blocked(query_single), blocked(key_float), blocked(value_float), blocked(decay_logarithm)),
    )
    return (outputs.reshape(length, head_count, value_width), carried_state)


def combine_states(earlier, latter):
    return (earlier[0] * latter[0], latter[0][:, :, None] * earlier[1] + latter[1])


def mixer_part(
    queries,
    key_rows,
    value_rows,
    forget_gate_input,
    channel_decay_rate,
    position_decay_factor,
    extra_log_decay,
    head_norm_gain,
    output_projection_weight,
):
    length = queries.shape[0]
    head_count = head_norm_gain.shape[0]
    query_single = queries.astype(jnp.float32).reshape(length, head_count, KEY_CHANNELS)
    key_float = key_rows.astype(jnp.float32).reshape(length, head_count, KEY_CHANNELS)
    value_float = value_rows.astype(jnp.float32).reshape(length, head_count, VALUE_DIM)
    gate_logarithm = jax.nn.log_sigmoid(forget_gate_input.astype(jnp.float32)).reshape(
        length, head_count, KEY_CHANNELS
    )
    decay_logarithm = (
        gate_logarithm
        * channel_decay_rate.reshape(head_count, KEY_CHANNELS)[None]
        * position_decay_factor[:, None, None]
        + extra_log_decay[:, :, None]
    )
    local_out, local_state = gla_blocks(query_single, key_float, value_float, decay_logarithm, SPAN)
    cumulative_decay = jnp.cumsum(decay_logarithm, axis=0)
    total_decay = jnp.exp(cumulative_decay[-1])
    identity = (jnp.ones_like(total_decay), jnp.zeros_like(local_state))
    incoming_state = carried_in((total_decay, local_state), EP, combine_states, identity)
    mixed_out = local_out + jnp.einsum(
        "pmj,mjx->pmx",
        query_single * jnp.exp(cumulative_decay),
        incoming_state[1],
        precision=highest_precision,
    )
    scale = lax.rsqrt(jnp.mean(mixed_out * mixed_out, axis=-1, keepdims=True) + norm_eps)
    head_normed = (
        (mixed_out * scale * head_norm_gain[None])
        .astype(jnp.bfloat16)
        .reshape(length, head_count * VALUE_DIM)
    )
    return sent_and_summed(
        jnp.dot(head_normed, output_projection_weight, preferred_element_type=jnp.float32).astype(
            jnp.bfloat16
        ),
        "tp",
        0,
    ).astype(jnp.bfloat16)


def expert_part(
    expert_input_rows,
    expert_norm_gain,
    routes,
    chosen_expert_weights,
    expert_gate_weight,
    expert_up_weight,
    expert_down_weight,
):
    token_count = expert_input_rows.shape[0]
    model_width = expert_input_rows.shape[1]
    top_count = routes.shape[1]
    rows_float = expert_input_rows.astype(jnp.float32)
    scaled = rows_float * lax.rsqrt(
        jnp.mean(rows_float * rows_float, axis=-1, keepdims=True) + norm_eps
    )
    moe_normed = (scaled * expert_norm_gain[None]).astype(jnp.bfloat16)
    expert_count = lax.axis_size(EP)
    capacity = 4 * token_count // expert_count
    flat_routes = routes.reshape(-1)
    onehot = (flat_routes[:, None] == jnp.arange(expert_count, dtype=jnp.int32)[None, :]).astype(
        jnp.int32
    )
    slot_ranks = jnp.cumsum(onehot, axis=0) - 1
    slot_index = jnp.sum(slot_ranks * onehot, axis=1)
    position = flat_routes * capacity + slot_index
    token_index = jnp.arange(token_count * top_count, dtype=jnp.int32) // top_count
    gate_weight = expert_gate_weight[0]
    up_weight = expert_up_weight[0]
    down_weight = expert_down_weight[0]
    buffer = (
        jnp.zeros((expert_count * capacity, model_width), jnp.bfloat16)
        .at[position]
        .set(moe_normed[token_index])
    )
    buffer = buffer.reshape(expert_count, capacity, model_width)
    arrived = lax.all_to_all(buffer, EP, split_axis=0, concat_axis=0, tiled=True)
    gate_sum = jnp.einsum("sid,df->sif", arrived, gate_weight, preferred_element_type=jnp.float32)
    up_sum = jnp.einsum("sid,df->sif", arrived, up_weight, preferred_element_type=jnp.float32)
    partial_value = jnp.einsum(
        "sif,fd->sid",
        (jax.nn.silu(gate_sum) * up_sum).astype(jnp.bfloat16),
        down_weight,
        preferred_element_type=jnp.float32,
    )
    summed = sent_and_summed(partial_value.astype(jnp.bfloat16), "tp", 2).astype(jnp.bfloat16)
    returned = lax.all_to_all(summed, EP, split_axis=0, concat_axis=0, tiled=True)
    flat_rows = returned.reshape(expert_count * capacity, returned.shape[2])
    picked = (
        flat_rows[position].astype(jnp.float32).reshape(token_count, top_count, returned.shape[2])
    )
    return jnp.sum(picked * chosen_expert_weights[:, :, None], axis=1).astype(jnp.bfloat16)


def body(
    queries,
    key_rows,
    value_rows,
    forget_gate_input,
    channel_decay_rate,
    position_decay_factor,
    extra_log_decay,
    head_norm_gain,
    output_projection_weight,
    expert_input_rows,
    expert_norm_gain,
    routes,
    chosen_expert_weights,
    expert_gate_weight,
    expert_up_weight,
    expert_down_weight,
):
    token_mixer_output = mixer_part(
        queries,
        key_rows,
        value_rows,
        forget_gate_input,
        channel_decay_rate,
        position_decay_factor,
        extra_log_decay,
        head_norm_gain,
        output_projection_weight,
    )
    moe_out = expert_part(
        expert_input_rows,
        expert_norm_gain,
        routes,
        chosen_expert_weights,
        expert_gate_weight,
        expert_up_weight,
        expert_down_weight,
    )
    return (token_mixer_output, moe_out)


def solution(mesh):
    finer = Mesh(mesh.devices.reshape(8, 4, 2, mesh.shape["tp"]), ("ep_0", "ep_1", "ep_2", "tp"))
    return jax.shard_map(
        body,
        mesh=finer,
        in_specs=(
            P(EP, "tp"),
            P(EP, "tp"),
            P(EP, "tp"),
            P(EP, "tp"),
            P("tp"),
            P(EP),
            P(EP, "tp"),
            P("tp", None),
            P("tp", None),
            P(EP, None),
            P(),
            P(EP, None),
            P(EP, None),
            P(EP, None, "tp"),
            P(EP, None, "tp"),
            P(EP, "tp", None),
        ),
        out_specs=(P(EP_TP, None), P(EP, "tp")),
        check_vma=False,
    )
```

profile of v0, /device:TPU:1, one launch (start us, length us, event | category | flops | bytes accessed | tf_op | source)
XLA Modules:
  0.0 284.7 jit_solution(10206821772801763680)
XLA Ops:
  6.1 2.5 fusion.27
  8.6 12.1 %scatter_custom_fusion = bf16[1024,2048]{1,0:T(8,128)(2,1)} fusion(s32[512]{0:T(512)S(1)} %bitcast.245, bf16[256,2048]{1,0:T(8,128)(2,1)} %fusion.27, s32[1024]{0:T(1024)S(1)} %pad_clamp_fusion.1, bf16[]{:T(256)} %constant.98.clone.1), kind=kCustom, calls=%fused_computation.46 | custom fusion | bytes 4194816 | tf_op jit(solution)/shard_map/scatter | solution.py:202
  20.7 13.5 %all-to-all-start.1 = ((bf16[64,16,2048]{2,1,0:T(8,128)(2,1)}), bf16[64,16,2048]{2,1,0:T(8,128)(2,1)}, u32[]{:S(2)}, u32[]{:S(2)}) async-start(bf16[64,16,2048]{2,1,0:T(8,128)(2,1)} %bitcast.219), calls=%async_computation.1 | async-start | bytes 8388608 | tf_op jit(solution)/shard_map/all_to_all | solution.py:205
  43.7 2.1 reshape.592
  45.7 2.1 reshape.593
  47.8 2.9 %multiply_add_fusion = f32[8,64,2,64]{3,2,1,0:T(2,128)} fusion(f32[8,64,2,64]{3,2,1,0:T(2,128)} %copy.89, f32[8,64,2]{2,1,0:T(8,128)} %bitcast.226, f32[8,64]{1,0:T(8,128)S(1)} %mul.390, f32[2,64]{1,0:T(2,128)S(1)} %mul.387), kind=kLoop, calls=%fused_computation.55 | loop fusion | flops 196608 | bytes 530944 | tf_op jit(solution)/shard_map/add | solution.py:138
  50.7 59.0 %while.13 = (s32[]{:T(128)}, f32[2,64,128]{2,1,0:T(8,128)S(1)}, f32[8,64,2,128]{3,1,0,2:T(8,128)}, f32[8,64,2,64]{3,2,1,0:T(2,128)}, f32[8,64,2,64]{3,2,1,0:T(2,...) while((s32[]{:T(128)}, f32[2,64,128]{2,1,0:T(8,128)S(1)}, ...), condition=%wide.region_3.4_spmd.clone, body=%wide.region_0.3_spmd.clone.sunk | while | flops 40988672 | bytes 1486964 | solution.py:106
  53.8 2.0 multiply_reduce_fusion.4
  61.2 2.0 multiply_reduce_fusion.4
  68.6 2.0 multiply_reduce_fusion.4
  76.0 2.0 multiply_reduce_fusion.4
  83.3 2.0 multiply_reduce_fusion.4
  111.5 4.5 %reduce-window.14 = f32[64,2,4,128]{3,0,1,2:T(8,128)S(1)} reduce-window(f32[64,2,4,128]{3,0,1,2:T(8,128)} %copy_bitcast_fusion.3, f32[]{:T(128)} %constant.82.clone.1), window={size=1x1x1x128 pad=0_0x0_0x0_0x127_0}, to_apply=%region_4.5 | reduce-window | flops 8323072 | bytes 524292 | tf_op jit(solution)/shard_map/reduce-window
  120.4 8.5 %all-to-all-done.1 = bf16[64,16,2048]{2,1,0:T(8,128)(2,1)} async-done(((bf16[64,16,2048]{2,1,0:T(8,128)(2,1)}), bf16[64,16,2048]{2,1,0:T(8,128)(2,1)}, u32[]{:S(2)}, u32[]{:S(2)}) %all-to-all-start.1) | async-done | bytes 4194336 | tf_op jit(solution)/shard_map/all_to_all | solution.py:205
  128.9 8.3 %fusion.19 = f32[64,16,768]{2,1,0:T(8,128)} fusion(bf16[64,16,2048]{2,1,0:T(8,128)(2,1)} %all-to-all-done.1, bf16[1,2048,768]{2,1,0:T(8,128)(2,1)} %param.32), kind=kOutput, calls=%fused_computation.35 | convolution fusion | flops 3221225472 | bytes 10485760 | tf_op jit(solution)/shard_map/sid,df->sif/dot_general | solution.py:207
  137.2 12.3 %convolution_convert_fusion = bf16[64,16,2048]{2,1,0:T(8,128)(2,1)} fusion(bf16[1,768,2048]{2,1,0:T(8,128)(2,1)S(1)} %copy-done, f32[64,16,768]{2,1,0:T(8,128)} %fusion.19, bf16[64,16,2048]{2,1,0:T(8,128)(2,1)} %all-to-all-done.1, bf16[1,2048,768]{2,1,0:T(8,128)(2,1)} %param.31), kind=kOutput, calls=%fused_computation.33 | convolution fusion | flops 6449266688 | bytes 17825792 | tf_op jit(solution)/shard_map/sif,fd->sid/dot_general | solution.py:208
  149.4 4.8 %copy.138 = bf16[64,2,4,8,512]{4,3,1,0,2:T(8,128)(2,1)} copy(bf16[64,2,4,8,512]{4,3,2,1,0:T(8,128)(2,1)} %bitcast.222) | data formatting | bytes 8388608 | tf_op jit(solution)/shard_map/reshape | solution.py:63
  154.3 4.9 %all-to-all-start.2 = ((bf16[4,64,16,512]{3,2,1,0:T(8,128)(2,1)}), bf16[4,64,16,512]{3,2,1,0:T(8,128)(2,1)}, u32[]{:S(2)}, u32[]{:S(2)}) async-start(bf16[4,64,16,512]{3,2,1,0:T(8,128)(2,1)} %bitcast.218), calls=%async_computation.2 | async-start | bytes 8388608 | tf_op jit(solution)/shard_map/all_to_all | solution.py:69
  160.9 9.9 %all-gather.4 = bf16[4,129,128]{2,1,0:T(8,128)(2,1)S(1)} all-gather(bf16[1,129,128]{2,1,0:T(8,128)(2,1)S(1)} %maximum_bitcast_fusion.1), channel_id=3, replica_groups=mesh['ep_0'=8,'ep_1'=4,'ep_2'=2,'tp'=4] {'ep_1'}, dimensions={0}, use_global_device_ids=true | all-gather | bytes 165120 | tf_op jit(solution)/shard_map/all_gather | solution.py:32
  174.8 23.2 %all-gather.5 = bf16[8,129,128]{2,1,0:T(8,128)(2,1)S(1)} all-gather(bf16[1,129,128]{2,1,0:T(8,128)(2,1)S(1)} %maximum_bitcast_fusion.2), channel_id=4, replica_groups=mesh['ep_0'=8,'ep_1'=4,'ep_2'=2,'tp'=4] {'ep_0'}, dimensions={0}, use_global_device_ids=true | all-gather | bytes 297216 | tf_op jit(solution)/shard_map/all_gather | solution.py:32
  199.5 2.1 copy.99
  204.1 2.2 multiply_reduce_fusion.2
  206.5 2.1 convolution_convert_fusion.1
  208.6 4.4 %all-to-all-start = ((bf16[4,128,2048]{2,1,0:T(8,128)(2,1)}), bf16[4,128,2048]{2,1,0:T(8,128)(2,1)}, u32[]{:S(2)}, u32[]{:S(2)}) async-start(bf16[4,128,2048]{2,1,0:T(8,128)(2,1)} %bitcast.220), calls=%async_computation | async-start | bytes 4194304 | tf_op jit(solution)/shard_map/all_to_all | solution.py:69
  213.1 4.4 %reduce_sum.76 = bf16[64,16,512]{2,1,0:T(8,128)(2,1)} reduce(bf16[4,64,16,512]{3,2,1,0:T(8,128)(2,1)} %all-to-all-done.2, bf16[]{:T(256)} %constant.98.clone.1), dimensions={0}, to_apply=%region_13.14 | reduce | flops 1572864 | bytes 5242882 | tf_op jit(solution)/shard_map/reduce_sum | solution.py:70
  217.5 15.2 %all-to-all-done = bf16[4,128,2048]{2,1,0:T(8,128)(2,1)} async-done(((bf16[4,128,2048]{2,1,0:T(8,128)(2,1)}), bf16[4,128,2048]{2,1,0:T(8,128)(2,1)}, u32[]{:S(2)}, u32[]{:S(2)}) %all-to-all-start) | async-done | bytes 2097184 | tf_op jit(solution)/shard_map/all_to_all | solution.py:69
  232.7 13.8 %all-to-all-start.3 = ((bf16[64,16,512]{2,1,0:T(8,128)(2,1)}), bf16[64,16,512]{2,1,0:T(8,128)(2,1)}, u32[]{:S(2)}, u32[]{:S(2)}) async-start(bf16[64,16,512]{2,1,0:T(8,128)(2,1)} %reduce_sum.76), calls=%async_computation.3 | async-start | bytes 2097152 | tf_op jit(solution)/shard_map/all_to_all | solution.py:215
  246.7 2.9 %reduce_sum.72 = bf16[128,2048]{1,0:T(8,128)(2,1)} reduce(bf16[4,128,2048]{2,1,0:T(8,128)(2,1)} %all-to-all-done, bf16[]{:T(256)} %constant.98.clone.1), dimensions={0}, to_apply=%region_7.8 | reduce | flops 786432 | bytes 2621442 | tf_op jit(solution)/shard_map/reduce_sum | solution.py:70
  249.6 25.0 %all-to-all-done.3 = bf16[64,16,512]{2,1,0:T(8,128)(2,1)} async-done(((bf16[64,16,512]{2,1,0:T(8,128)(2,1)}), bf16[64,16,512]{2,1,0:T(8,128)(2,1)}, u32[]{:S(2)}, u32[]{:S(2)}) %all-to-all-start.3) | async-done | bytes 1048608 | tf_op jit(solution)/shard_map/all_to_all | solution.py:215
  274.6 4.0 %gather_fusion = bf16[512,512]{1,0:T(8,128)(2,1)} fusion(bf16[1024,512]{1,0:T(8,128)(2,1)} %bitcast.54, s32[1024]{0:T(1024)S(1)} %pad_clamp_fusion), kind=kCustom, calls=%fused_computation.1 | custom fusion | bytes 1050624 | tf_op jit(solution)/shard_map/gather | solution.py:218
  278.7 2.7 reshape.631
  281.3 3.3 %multiply_reduce_fusion.1 = bf16[256,512]{1,0:T(8,128)(2,1)} fusion(f32[256,2,512]{2,1,0:T(2,128)} %reshape.631, f32[256,2]{1,0:T(8,128)S(1)} %copy.105), kind=kLoop, calls=%fused_computation.51 | loop fusion | flops 393216 | bytes 1312768 | tf_op jit(solution)/shard_map/reduce_sum | solution.py:220
  (202 shorter events, 79.0 us)
Async XLA Ops:
  0.6 136.5 %copy-start = (bf16[1,768,2048]{2,1,0:T(8,128)(2,1)S(1)}, bf16[1,768,2048]{2,1,0:T(8,128)(2,1)}, u32[]{:S(2)}) copy-start(bf16[1,768,2048]{2,1,0:T(8,128)(2,1)} %param.33) | copy-start | bytes 9437188
  20.7 13.5 %copy-start.5 = (bf16[512,128]{1,0:T(8,128)(2,1)S(1)}, bf16[512,128]{1,0:T(8,128)(2,1)}, u32[]{:S(2)}) copy-start(bf16[512,128]{1,0:T(8,128)(2,1)} %param.21) | copy-start | bytes 393220
  20.7 15.4 %copy-start.10 = (f32[128]{0:T(128)S(1)}, f32[128]{0:T(128)}, u32[]{:S(2)}) copy-start(f32[128]{0:T(128)} %param.22) | copy-start | bytes 1540
  20.7 18.5 %copy-start.6 = (f32[512,2]{0,1:T(2,128)S(1)}, f32[512,2]{0,1:T(2,128)}, u32[]{:S(2)}) copy-start(f32[512,2]{0,1:T(2,128)} %param.24) | copy-start | bytes 12292
  20.7 19.3 %copy-start.7 = (f32[512]{0:T(512)S(1)}, f32[512]{0:T(512)}, u32[]{:S(2)}) copy-start(f32[512]{0:T(512)} %param.23) | copy-start | bytes 6148
  20.7 108.2 %all-to-all-start.1 = ((bf16[64,16,2048]{2,1,0:T(8,128)(2,1)}), bf16[64,16,2048]{2,1,0:T(8,128)(2,1)}, u32[]{:S(2)}, u32[]{:S(2)}) async-start(bf16[64,16,2048]{2,1,0:T(8,128)(2,1)} %bitcast.219), calls=%async_computation.1 | async-start | bytes 8388608 | tf_op jit(solution)/shard_map/all_to_all | solution.py:205
  36.1 14.6 %copy-start.1 = (f32[512,128]{0,1:T(8,128)}, f32[512,128]{0,1:T(8,128)S(1)}, u32[]{:S(2)}) copy-start(f32[512,128]{0,1:T(8,128)S(1)} %fusion.34) | copy-start | bytes 786436
  154.3 54.3 %all-to-all-start.2 = ((bf16[4,64,16,512]{3,2,1,0:T(8,128)(2,1)}), bf16[4,64,16,512]{3,2,1,0:T(8,128)(2,1)}, u32[]{:S(2)}, u32[]{:S(2)}) async-start(bf16[4,64,16,512]{3,2,1,0:T(8,128)(2,1)} %bitcast.218), calls=%async_computation.2 | async-start | bytes 8388608 | tf_op jit(solution)/shard_map/all_to_all | solution.py:69
  159.1 47.2 %copy-start.9 = (f32[2,128]{1,0:T(2,128)S(1)}, f32[2,128]{1,0:T(2,128)}, u32[]{:S(2)}) copy-start(f32[2,128]{1,0:T(2,128)} %param.25) | copy-start | bytes 3076
  170.8 0.7 copy-start.2
  198.1 0.7 copy-start.3
  201.5 4.9 %copy-start.4 = (bf16[256,2048]{1,0:T(8,128)(2,1)S(1)}, bf16[256,2048]{1,0:T(8,128)(2,1)}, u32[]{:S(2)}) copy-start(bf16[256,2048]{1,0:T(8,128)(2,1)} %param.26) | copy-start | bytes 3145732
  208.6 24.1 %all-to-all-start = ((bf16[4,128,2048]{2,1,0:T(8,128)(2,1)}), bf16[4,128,2048]{2,1,0:T(8,128)(2,1)}, u32[]{:S(2)}, u32[]{:S(2)}) async-start(bf16[4,128,2048]{2,1,0:T(8,128)(2,1)} %bitcast.220), calls=%async_computation | async-start | bytes 4194304 | tf_op jit(solution)/shard_map/all_to_all | solution.py:69
  213.0 33.5 %copy-start.8 = (f32[256,2]{0,1:T(2,128)S(1)}, f32[256,2]{0,1:T(2,128)}, u32[]{:S(2)}) copy-start(f32[256,2]{0,1:T(2,128)} %param.30) | copy-start | bytes 6148
  232.7 41.9 %all-to-all-start.3 = ((bf16[64,16,512]{2,1,0:T(8,128)(2,1)}), bf16[64,16,512]{2,1,0:T(8,128)(2,1)}, u32[]{:S(2)}, u32[]{:S(2)}) async-start(bf16[64,16,512]{2,1,0:T(8,128)(2,1)} %reduce_sum.76), calls=%async_computation.3 | async-start | bytes 2097152 | tf_op jit(solution)/shard_map/all_to_all | solution.py:215
where the time goes:
time: 288 us; the launch traced here: 285 us
  other arithmetic  63.9 us (22%)
  local copies, waits for them, and re-layouts  63.2 us (22%)
  waiting for transfers between devices  48.7 us (17%)
  starting transfers between devices  36.6 us (13%)
  matrix products  35.5 us (12%)
  blocking collectives  35.2 us (12%)
    all_gather x3, blocking collectives, gathered_once(): both, at, found = (lax.all_gather(jnp.concatenate(lines), axis), 0, {})  35.2 us
    all_to_all x1, waiting for transfers between devices, expert_part(): lax.all_to_all(summed, EP, split_axis=0, concat_axis=0, tiled=True)  25 us
    reduce_sum x8, other arithmetic, advance(): jnp.sum(block_queries[:, None] * block_keys[None, :] * decays, axis=-1)  16.4 us
    dynamic_slice x24, local copies, waits for them, and re-layouts, gla_blocks(): lax.scan(advance, start_state, (blocked(query_single), blocked(key_float)...  16.3 us
    all_to_all x2, waiting for transfers between devices, sent_and_summed(): lax.all_to_all(tiles, axis, split_axis=0, concat_axis=0, tiled=True)  15.2 us
    all_to_all x1, starting transfers between devices, expert_part(): lax.all_to_all(summed, EP, split_axis=0, concat_axis=0, tiled=True)  13.8 us
    all_to_all x1, starting transfers between devices, expert_part(): lax.all_to_all(buffer, EP, split_axis=0, concat_axis=0, tiled=True)  13.5 us
    dot_general x1, matrix products, expert_part(): jnp.einsum('sif,fd->sid', (jax.nn.silu(gate_sum) * up_sum).astype(jnp.bfl...  12.3 us
  transfers between devices with their start and end apart: 4, of which 3 were waited for; matrix products, arithmetic and copies ran while one was open for 37% of the time, Pallas kernels for 0%

commit v1 on v0

v1 whole, which is shorter than its diff:
```python
import functools

import jax
import jax.numpy as jnp
from jax import lax
from jax.experimental import pallas as pl
from jax.experimental.pallas import tpu as pltpu
from jax.sharding import Mesh
from jax.sharding import PartitionSpec as P

F32, BF16 = jnp.float32, jnp.bfloat16
MESH = pl.DeviceIdType.MESH
NX = 4
CAP = 16
BLOCK = 128
LEVELS = (64, 32, 16, 8, 4, 2, 1)
EPS = 1e-06
EP = ("z", "yc")
EP_TP = ("z", "yc", "tp")


def dot(a, b):
    return jnp.dot(a, b, preferred_element_type=F32)


def dot_nt(a, b):
    return lax.dot_general(a, b, (((1,), (1,)), ((), ())), preferred_element_type=F32)


def dot_tn(a, b):
    return lax.dot_general(a, b, (((0,), (0,)), ((), ())), preferred_element_type=F32)


def iota(shape, dim):
    return lax.broadcasted_iota(jnp.int32, shape, dim)


def one_where(mask):
    return jnp.where(mask, 1.0, 0.0)


def away_order(count):
    order = [0]
    for d in range(1, count // 2 + 1):
        for e in (d, count - d):
            if e not in order:
                order.append(e)
    return order


def kernel(
    nz,
    nyc,
    per_chunk,
    routes,
    routes_t,
    chosen,
    rows,
    gain,
    queries,
    keys,
    values,
    log_decay,
    head_gain,
    out_weight,
    gate_hbm,
    up_hbm,
    down_hbm,
    mix_out,
    moe_out,
    gate_w,
    up_w,
    down_w,
    weight_sem,
    zsnd,
    zin,
    xq,
    part,
    pass_a,
    pass_b,
    from_left,
    from_right,
    result,
    yin,
    zret,
    zs,
    zr,
    ys,
    yr,
    xs,
    xr,
    ps,
    pr,
    y2s,
    y2r,
    z2s,
    z2r,
    sums,
    local_out,
    decayed_q,
    state,
    total,
    normed,
    sy,
    tz,
    sz,
    incoming,
    before,
    sys_,
    syr,
    szs,
    szr,
    mp,
    mpa,
    mpb,
    mq1,
    mq3,
    ms,
    mr,
):
    z, yc, x = lax.axis_index("z"), lax.axis_index("yc"), lax.axis_index("tp")
    right, left = lax.rem(x + 1, NX), lax.rem(x + NX - 1, NX)
    order = away_order(nz)
    zrows = nyc * CAP
    half = zrows // 2
    quarter = rows.shape[1] // NX
    tokens = rows.shape[0]
    length = queries.shape[0]
    blocks = length // BLOCK
    chunks = nz // per_chunk
    crows = per_chunk * zrows

    def remote(src, dst, send, recv, device):
        return pltpu.make_async_remote_copy(
            src_ref=src, dst_ref=dst, send_sem=send, recv_sem=recv, device_id=device, device_id_type=MESH
        )

    def arrived(ref, sem):
        pltpu.make_async_copy(ref, ref, sem).wait()

    def times(value, unit):
        return pl.multiple_of(value * unit, unit)

    def columns(r):
        return pl.ds(r * quarter, quarter)

    loads = []
    for r in range(NX):
        back = times(lax.rem(x + NX - r, NX), quarter)
        ahead = times(lax.rem(x + r, NX), quarter)
        loads += [
            pltpu.make_async_copy(gate_hbm.at[0, pl.ds(back, quarter), :], gate_w.at[columns(r), :], weight_sem.at[3 * r]),
            pltpu.make_async_copy(up_hbm.at[0, pl.ds(back, quarter), :], up_w.at[columns(r), :], weight_sem.at[3 * r + 1]),
            pltpu.make_async_copy(down_hbm.at[0, :, pl.ds(ahead, quarter)], down_w.at[:, columns(r)], weight_sem.at[3 * r + 2]),
        ]
    for load in loads:
        load.start()

    barrier = pltpu.get_barrier_semaphore()
    pl.semaphore_signal(barrier, inc=1, device_id={"tp": right}, device_id_type=MESH)
    pl.semaphore_signal(barrier, inc=1, device_id={"tp": left}, device_id_type=MESH)

    def greet_z(t, carry):
        pl.semaphore_signal(barrier, inc=1, device_id={"z": lax.rem(z + t, nz)}, device_id_type=MESH)
        return carry

    def greet_y(t, carry):
        pl.semaphore_signal(barrier, inc=1, device_id={"yc": lax.rem(yc + t, nyc)}, device_id_type=MESH)
        return carry

    lax.fori_loop(1, nz, greet_z, 0)
    lax.fori_loop(1, nyc, greet_y, 0)

    experts = nz * nyc
    first_t, second_t = routes_t[0:1, :], routes_t[1:2, :]
    marks = [one_where(iota((experts, tokens), 0) == e) for e in (first_t, second_t)]
    upper = one_where(iota((tokens, tokens), 0) < iota((tokens, tokens), 1)).astype(BF16)
    ranks = [dot(m.astype(BF16), upper) for m in marks]
    ranks[1] = ranks[1] + jnp.sum(marks[0], axis=1, keepdims=True)
    slots_t = [
        e.astype(F32) * CAP + jnp.sum(m * r, axis=0, keepdims=True)
        for e, m, r in zip((first_t, second_t), marks, ranks)
    ]

    own = times(x, quarter)
    squares = rows[...].astype(F32)
    scale = lax.rsqrt(jnp.mean(squares * squares, axis=1, keepdims=True) + EPS)
    moe_normed = (rows[:, pl.ds(own, quarter)].astype(F32) * scale * gain[:, pl.ds(own, quarter)]).astype(BF16)

    pl.semaphore_wait(barrier, 2 + (nz - 1) + (nyc - 1))

    for k, d in enumerate(order):
        base = lax.rem(z + d, nz) * zrows
        slot = (iota((zrows, tokens), 0) + base).astype(F32)
        chooser = one_where((slot == slots_t[0]) | (slot == slots_t[1])).astype(BF16)
        zsnd[k] = dot(chooser, moe_normed).astype(BF16)
        if k:
            remote(zsnd.at[k], zin.at[k], zs.at[k], zr.at[k], {"z": lax.rem(z + d, nz)}).start()

    def forward_y(k):
        source = zin if k else zsnd
        if k:
            arrived(zin.at[k], zr.at[k])

        def send(t, carry):
            to = lax.rem(yc + t, nyc)
            remote(
                source.at[k, pl.ds(times(to, CAP), CAP), :],
                xq.at[pl.ds(pl.multiple_of(k * zrows + yc * CAP, CAP), CAP), columns(0)],
                ys.at[k],
                yr.at[k],
                {"yc": to},
            ).start()
            return carry

        lax.fori_loop(1, nyc, send, 0)
        xq[pl.ds(pl.multiple_of(k * zrows + yc * CAP, CAP), CAP), columns(0)] = source[k, pl.ds(times(yc, CAP), CAP), :]

    def forward_x(k):
        mine = xq.at[pl.ds(k * zrows, zrows), columns(0)]
        arrived(xq.at[pl.ds(k * zrows, zrows - CAP), columns(0)], yr.at[k])
        remote(mine, xq.at[pl.ds(k * zrows, zrows), columns(1)], xs.at[0, k], xr.at[0, k], {"tp": right}).start()
        remote(mine, xq.at[pl.ds(k * zrows, zrows), columns(3)], xs.at[1, k], xr.at[1, k], {"tp": left}).start()

    def relay(k):
        a, b = pl.ds(k * zrows, half), pl.ds(k * zrows + half, half)
        arrived(xq.at[pl.ds(k * zrows, zrows), columns(1)], xr.at[0, k])
        remote(xq.at[a, columns(1)], xq.at[a, columns(2)], xs.at[2, k], xr.at[2, k], {"tp": right}).start()
        arrived(xq.at[pl.ds(k * zrows, zrows), columns(3)], xr.at[1, k])
        remote(xq.at[b, columns(3)], xq.at[b, columns(2)], xs.at[3, k], xr.at[3, k], {"tp": left}).start()

    chalf = crows // 2

    def expert(c):
        for k in range(c * per_chunk, (c + 1) * per_chunk):
            arrived(xq.at[pl.ds(k * zrows, half), columns(2)], xr.at[2, k])
            arrived(xq.at[pl.ds(k * zrows + half, half), columns(2)], xr.at[3, k])
        if c == 0:
            for load in loads:
                load.wait()
        here = pl.ds(c * crows, crows)
        gate = dot(xq[here, :], gate_w[...])
        up = dot(xq[here, :], up_w[...])
        hidden = (jax.nn.silu(gate) * up).astype(BF16)
        part[here, :] = dot(hidden, down_w[...]).astype(BF16)
        a, b = pl.ds(c * crows, chalf), pl.ds(c * crows + chalf, chalf)
        remote(part.at[a, columns(2)], pass_a.at[c], ps.at[0, c], pr.at[0, c], {"tp": right}).start()
        remote(part.at[b, columns(2)], pass_b.at[c], ps.at[1, c], pr.at[1, c], {"tp": left}).start()

    def add_pass(c):
        here = pl.ds(c * crows, crows)
        a, b = pl.ds(c * crows, chalf), pl.ds(c * crows + chalf, chalf)
        arrived(pass_a.at[c], pr.at[0, c])
        part[a, columns(1)] = (part[a, columns(1)].astype(F32) + pass_a[c].astype(F32)).astype(BF16)
        remote(part.at[here, columns(1)], from_left.at[here], ps.at[2, c], pr.at[2, c], {"tp": right}).start()
        arrived(pass_b.at[c], pr.at[1, c])
        part[b, columns(3)] = (part[b, columns(3)].astype(F32) + pass_b[c].astype(F32)).astype(BF16)
        remote(part.at[here, columns(3)], from_right.at[here], ps.at[3, c], pr.at[3, c], {"tp": left}).start()

    def give_back_y(c):
        here = pl.ds(c * crows, crows)
        arrived(from_left.at[here], pr.at[2, c])
        arrived(from_right.at[here], pr.at[3, c])
        result[here, :] = (
            part[here, columns(0)].astype(F32) + from_left[here, :].astype(F32) + from_right[here, :].astype(F32)
        ).astype(BF16)
        for k in range(c * per_chunk, (c + 1) * per_chunk):

            def send(t, carry):
                to = lax.rem(yc + t, nyc)
                remote(
                    result.at[pl.ds(pl.multiple_of(k * zrows + to * CAP, CAP), CAP), :],
                    yin.at[k, pl.ds(times(yc, CAP), CAP), :],
                    y2s.at[k],
                    y2r.at[k],
                    {"yc": to},
                ).start()
                return carry

            lax.fori_loop(1, nyc, send, 0)
            yin[k, pl.ds(times(yc, CAP), CAP), :] = result[pl.ds(pl.multiple_of(k * zrows + yc * CAP, CAP), CAP), :]

    def give_back_z(c):
        for k in range(c * per_chunk, (c + 1) * per_chunk):
            arrived(yin.at[k, pl.ds(0, zrows - CAP), :], y2r.at[k])
            if k:
                to = lax.rem(z + nz - order[k], nz)
                remote(yin.at[k], zret.at[k], z2s.at[k], z2r.at[k], {"z": to}).start()

    def combine():
        first, second = routes[:, 0:1], routes[:, 1:2]
        marks = [one_where(iota((tokens, experts), 1) == e) for e in (first, second)]
        lower = one_where(iota((tokens, tokens), 0) > iota((tokens, tokens), 1)).astype(BF16)
        ranks = [dot(lower, m.astype(BF16)) for m in marks]
        ranks[1] = ranks[1] + jnp.sum(marks[0], axis=0, keepdims=True)
        slots = [
            e.astype(F32) * CAP + jnp.sum(m * r, axis=1, keepdims=True)
            for e, m, r in zip((first, second), marks, ranks)
        ]
        mixed = jnp.zeros((tokens, quarter), F32)
        for k, d in enumerate(order):
            base = lax.rem(z + d, nz) * zrows
            slot = (iota((tokens, zrows), 1) + base).astype(F32)
            weight = jnp.where(slot == slots[0], chosen[:, 0:1], 0.0) + jnp.where(slot == slots[1], chosen[:, 1:2], 0.0)
            high = weight.astype(BF16)
            low = (weight - high.astype(F32)).astype(BF16)
            if k:
                arrived(zret.at[k], z2r.at[k])
            returned = zret[k] if k else yin[k]
            mixed = mixed + dot(high, returned) + dot(low, returned)
        moe_out[...] = mixed.astype(BF16)

    def prepare_sums():
        i, j = iota((BLOCK, BLOCK), 0), iota((BLOCK, BLOCK), 1)
        for level, h in enumerate(LEVELS):
            edge = (i & ~(2 * h - 1)) + h
            after = (j >= edge) & (j <= i)
            ahead = (j > i) & (j < edge)
            m = one_where(after | ahead).astype(BF16)
            sums[pl.ds(level * BLOCK, BLOCK), pl.ds(0, BLOCK)] = m
            sums[pl.ds(level * BLOCK, BLOCK), pl.ds(BLOCK, BLOCK)] = m
        for level, m in ((len(LEVELS), j <= i), (len(LEVELS) + 1, j > i)):
            m = one_where(m).astype(BF16)
            sums[pl.ds(level * BLOCK, BLOCK), pl.ds(0, BLOCK)] = m
            sums[pl.ds(level * BLOCK, BLOCK), pl.ds(BLOCK, BLOCK)] = m

    first_head = iota((BLOCK, BLOCK), 1) < BLOCK // 2

    def by_head(value):
        return jnp.concatenate([jnp.where(first_head, value, 0.0), jnp.where(first_head, 0.0, value)], axis=0).astype(BF16)

    def gla_block(b):
        r = pl.ds(b * BLOCK, BLOCK)
        g = log_decay[r, :]
        high = g.astype(BF16)
        low = (g - high.astype(F32)).astype(BF16)
        e = jnp.exp(dot(sums[...], jnp.concatenate([high, low], axis=0)))
        q, k = queries[r, :].astype(F32), keys[r, :].astype(F32)
        i, j = iota((BLOCK, 2 * BLOCK), 0), iota((BLOCK, 2 * BLOCK), 1) & (BLOCK - 1)
        apart = i ^ j
        scores = None
        for level, h in enumerate(LEVELS):
            factor = e[level * BLOCK : (level + 1) * BLOCK]
            s = dot_nt((q * factor).astype(BF16), by_head(k * factor))
            scores = s if scores is None else jnp.where(apart < 2 * h, s, scores)
        scores = jnp.where(apart < 1, dot_nt(queries[r, :], by_head(k)), scores)
        scores = jnp.where(i >= j, scores, 0.0).astype(BF16)
        n = len(LEVELS)
        from_start = e[n * BLOCK : (n + 1) * BLOCK]
        to_end = e[(n + 1) * BLOCK : (n + 2) * BLOCK]
        qg = q * from_start
        outs = [
            dot(scores[:, h * BLOCK : (h + 1) * BLOCK], values[r, pl.ds(h * BLOCK, BLOCK)]) for h in range(2)
        ]
        if b:
            carried = dot_nt(by_head(qg), state[...].astype(BF16))
            outs = [o + carried[h * BLOCK : (h + 1) * BLOCK] for h, o in enumerate(outs)]
            decayed_q[r, :] = (qg * total[...]).astype(BF16)
        else:
            decayed_q[r, :] = qg.astype(BF16)
        for h in range(2):
            local_out[r, pl.ds(h * BLOCK, BLOCK)] = outs[h]
        grown = dot_tn(values[r, :], (k * to_end).astype(BF16))
        fresh = jnp.where(first_head, grown[0:BLOCK], grown[BLOCK : 2 * BLOCK])
        through = from_start[BLOCK - 1 : BLOCK, :]
        if b:
            state[...] = state[...] * through + fresh
            total[...] = total[...] * through
        else:
            state[...] = fresh
            total[...] = through

    def packed(s, d):
        high = d.astype(BF16).astype(F32)
        row = iota((16, BLOCK), 0)
        tail = jnp.where(row == 0, high, jnp.where(row == 1, d - high, 0.0))
        return s.astype(BF16), tail.astype(BF16)

    def opened(ref, at):
        tail = ref[at, pl.ds(BLOCK, 16), :].astype(F32)
        return ref[at, pl.ds(0, BLOCK), :].astype(F32), tail[0:1] + tail[1:2]

    def states_y():
        s, tail = packed(state[...], total[...])
        tz[1, pl.ds(0, BLOCK), :] = s
        tz[1, pl.ds(BLOCK, 16), :] = tail

        def send(t, carry):
            to = lax.rem(yc + t, nyc)
            remote(tz.at[1], sy.at[yc], sys_, syr, {"yc": to}).start()
            return carry

        lax.fori_loop(1, nyc, send, 0)
        sy[yc, pl.ds(0, BLOCK), :] = s
        sy[yc, pl.ds(BLOCK, 16), :] = tail

    def states_z():
        arrived(sy.at[pl.ds(0, nyc - 1)], syr)
        run_s, run_d = jnp.zeros((BLOCK, BLOCK), F32), jnp.ones((1, BLOCK), F32)
        before[pl.ds(0, BLOCK), :] = run_s
        before[pl.ds(BLOCK, 8), :] = jnp.broadcast_to(run_d, (8, BLOCK))
        for s in range(nyc):
            new_s, new_d = opened(sy, s)
            run_s, run_d = run_s * new_d + new_s, run_d * new_d

            @pl.when(s < yc)
            def _(run_s=run_s, run_d=run_d):
                before[pl.ds(0, BLOCK), :] = run_s
                before[pl.ds(BLOCK, 8), :] = jnp.broadcast_to(run_d, (8, BLOCK))

        s, tail = packed(run_s, run_d)
        tz[0, pl.ds(0, BLOCK), :] = s
        tz[0, pl.ds(BLOCK, 16), :] = tail
        for d in range(1, nz):

            @pl.when(z + d < nz)
            def _(d=d):
                remote(tz.at[0], sz.at[z], szs.at[d], szr.at[z], {"z": z + d}).start()

    def states_in():
        incoming[...] = jnp.zeros((BLOCK, BLOCK), F32)
        for s in range(nz - 1):

            @pl.when(s < z)
            def _(s=s):
                arrived(sz.at[s], szr.at[s])
                new_s, new_d = opened(sz, s)
                incoming[...] = incoming[...] * new_d + new_s

        incoming[...] = incoming[...] * before[pl.ds(BLOCK, 8), :][0:1] + before[pl.ds(0, BLOCK), :]

    mrows = length // NX
    mhalf = mrows // 2

    def mix():
        s = incoming[...].astype(BF16)
        for b in range(blocks):
            r = pl.ds(b * BLOCK, BLOCK)
            carried = dot_nt(by_head(decayed_q[r, :].astype(F32)), s)
            for h in range(2):
                c = pl.ds(h * BLOCK, BLOCK)
                o = local_out[r, c] + carried[h * BLOCK : (h + 1) * BLOCK]
                o = o * lax.rsqrt(jnp.mean(o * o, axis=1, keepdims=True) + EPS) * head_gain[h : h + 1, :]
                normed[r, c] = o.astype(BF16)
        for r in (2, 1, 3, 0):
            to = times(lax.rem(x + r, NX), mrows)
            mp[r] = dot(normed[pl.ds(to, mrows), :], out_weight[...]).astype(BF16)
            if r == 2:
                remote(mp.at[2, pl.ds(0, mhalf)], mpa, ms.at[0], mr.at[0], {"tp": right}).start()
                remote(mp.at[2, pl.ds(mhalf, mhalf)], mpb, ms.at[1], mr.at[1], {"tp": left}).start()

    def mix_pass():
        a, b = pl.ds(0, mhalf), pl.ds(mhalf, mhalf)
        arrived(mpa, mr.at[0])
        mp[1, a] = (mp[1, a].astype(F32) + mpa[...].astype(F32)).astype(BF16)
        remote(mp.at[1], mq1, ms.at[2], mr.at[2], {"tp": right}).start()
        arrived(mpb, mr.at[1])
        mp[3, b] = (mp[3, b].astype(F32) + mpb[...].astype(F32)).astype(BF16)
        remote(mp.at[3], mq3, ms.at[3], mr.at[3], {"tp": left}).start()

    def mix_end():
        arrived(mq1, mr.at[2])
        arrived(mq3, mr.at[3])
        mix_out[...] = (mp[0].astype(F32) + mq1[...].astype(F32) + mq3[...].astype(F32)).astype(BF16)

    def step(work, index, count):
        if 0 <= index < count:
            work(index)

    prepare_sums()
    settle = per_chunk + 2
    last = settle + per_chunk * (chunks - 1) + 3
    for s in range(last + 1):
        step(forward_y, s, nz)
        step(forward_x, s - 1, nz)
        step(relay, s - 2, nz)
        for lag, work in ((3, give_back_z), (2, give_back_y), (1, add_pass), (0, expert)):
            at = s - settle - lag
            if at % per_chunk == 0:
                step(work, at // per_chunk, chunks)
        step(gla_block, s, blocks)
        if s == blocks - 1:
            states_y()
        if s == blocks + 1:
            states_z()
        if s == blocks + 3:
            states_in()
            mix()
        if s == blocks + 5:
            mix_pass()
        if s == blocks + 7:
            mix_end()
    if last < blocks + 3:
        states_in()
        mix()
    if last < blocks + 5:
        mix_pass()
    if last < blocks + 7:
        mix_end()
    combine()

    for k in range(nz):
        arrived(xq.at[pl.ds(0, zrows - CAP), columns(0)], ys.at[k])
        arrived(yin.at[0, pl.ds(0, zrows - CAP), :], y2s.at[k])
        if k:
            arrived(zsnd.at[k], zs.at[k])
            arrived(yin.at[k], z2s.at[k])
        for side in range(2):
            arrived(xq.at[pl.ds(0, zrows), columns(0)], xs.at[side, k])
            arrived(xq.at[pl.ds(0, half), columns(0)], xs.at[2 + side, k])
    for c in range(chunks):
        for side in range(2):
            arrived(pass_a.at[c], ps.at[side, c])
            arrived(from_left.at[pl.ds(0, crows)], ps.at[2 + side, c])
    arrived(sy.at[pl.ds(0, nyc - 1)], sys_)
    for d in range(1, nz):

        @pl.when(z + d < nz)
        def _(d=d):
            arrived(tz.at[0], szs.at[d])

    for side in range(2):
        arrived(mpa, ms.at[side])
        arrived(mq1, ms.at[2 + side])


def body(
    nz,
    nyc,
    per_chunk,
    queries,
    key_rows,
    value_rows,
    forget_gate_input,
    channel_decay_rate,
    position_decay_factor,
    extra_log_decay,
    head_norm_gain,
    output_projection_weight,
    expert_input_rows,
    expert_norm_gain,
    routes,
    chosen_expert_weights,
    expert_gate_weight,
    expert_up_weight,
    expert_down_weight,
):
    length, channels = queries.shape
    tokens, width = expert_input_rows.shape
    hidden = expert_gate_weight.shape[2]
    quarter = width // NX
    zrows = nyc * CAP
    crows = per_chunk * zrows
    chunks = nz // per_chunk
    heads = extra_log_decay.shape[1]
    extra = jnp.where(
        lax.broadcasted_iota(jnp.int32, (length, channels), 1) < channels // heads,
        extra_log_decay[:, 0:1],
        extra_log_decay[:, 1:2],
    )
    log_decay = (
        jax.nn.log_sigmoid(forget_gate_input.astype(F32)) * channel_decay_rate[None, :] * position_decay_factor[:, None]
        + extra
    )
    dma, vmem = pltpu.SemaphoreType.DMA, pltpu.VMEM
    mrows = length // NX
    return pl.pallas_call(
        functools.partial(kernel, nz, nyc, per_chunk),
        out_shape=(
            jax.ShapeDtypeStruct((mrows, width), BF16),
            jax.ShapeDtypeStruct((tokens, quarter), BF16),
        ),
        in_specs=[pl.BlockSpec(memory_space=vmem)] * 11 + [pl.BlockSpec(memory_space=pl.ANY)] * 3,
        out_specs=(pl.BlockSpec(memory_space=vmem), pl.BlockSpec(memory_space=vmem)),
        scratch_shapes=[
            vmem((width, hidden), BF16),
            vmem((width, hidden), BF16),
            vmem((hidden, width), BF16),
            dma((3 * NX,)),
            vmem((nz, zrows, quarter), BF16),
            vmem((nz, zrows, quarter), BF16),
            vmem((nz * zrows, width), BF16),
            vmem((nz * zrows, width), BF16),
            vmem((chunks, crows // 2, quarter), BF16),
            vmem((chunks, crows // 2, quarter), BF16),
            vmem((nz * zrows, quarter), BF16),
            vmem((nz * zrows, quarter), BF16),
            vmem((nz * zrows, quarter), BF16),
            vmem((nz, zrows, quarter), BF16),
            vmem((nz, zrows, quarter), BF16),
            dma((nz,)),
            dma((nz,)),
            dma((nz,)),
            dma((nz,)),
            dma((4, nz)),
            dma((4, nz)),
            dma((4, chunks)),
            dma((4, chunks)),
            dma((nz,)),
            dma((nz,)),
            dma((nz,)),
            dma((nz,)),
            vmem(((len(LEVELS) + 2) * BLOCK, 2 * BLOCK), BF16),
            vmem((length, 2 * BLOCK), F32),
            vmem((length, BLOCK), BF16),
            vmem((BLOCK, BLOCK), F32),
            vmem((1, BLOCK), F32),
            vmem((length, 2 * BLOCK), BF16),
            vmem((nyc, BLOCK + 16, BLOCK), BF16),
            vmem((2, BLOCK + 16, BLOCK), BF16),
            vmem((nz, BLOCK + 16, BLOCK), BF16),
            vmem((BLOCK, BLOCK), F32),
            vmem((BLOCK + 8, BLOCK), F32),
            dma(()),
            dma(()),
            dma((nz,)),
            dma((nz,)),
            vmem((NX, mrows, width), BF16),
            vmem((mrows // 2, width), BF16),
            vmem((mrows // 2, width), BF16),
            vmem((mrows, width), BF16),
            vmem((mrows, width), BF16),
            dma((4,)),
            dma((4,)),
        ],
        compiler_params=pltpu.CompilerParams(
            collective_id=0, has_side_effects=True, vmem_limit_bytes=60 * 1024 * 1024
        ),
        name="mixer_and_experts",
    )(
        routes,
        routes.T,
        chosen_expert_weights,
        expert_input_rows,
        expert_norm_gain[None, :],
        queries,
        key_rows,
        value_rows,
        log_decay,
        head_norm_gain,
        output_projection_weight,
        expert_gate_weight,
        expert_up_weight,
        expert_down_weight,
    )


def mapped(mesh, nz, nyc, per_chunk):
    finer = Mesh(mesh.devices.reshape(nz, nyc, NX), EP_TP)
    return jax.shard_map(
        functools.partial(body, nz, nyc, per_chunk),
        mesh=finer,
        in_specs=(
            P(EP, "tp"),
            P(EP, "tp"),
            P(EP, "tp"),
            P(EP, "tp"),
            P("tp"),
            P(EP),
            P(EP, "tp"),
            P("tp", None),
            P("tp", None),
            P(EP, None),
            P(),
            P(EP, None),
            P(EP, None),
            P(EP, None, "tp"),
            P(EP, None, "tp"),
            P(EP, "tp", None),
        ),
        out_specs=(P(EP_TP, None), P(EP, "tp")),
        check_vma=False,
    )


def solution(mesh):
    return mapped(mesh, 8, 8, 2)
```

time: 288 us -> 142 us (0.49)
  Pallas kernels: 0 us -> 131 us
  other arithmetic: 63.9 us -> 1.9 us
  local copies, waits for them, and re-layouts: 63.2 us -> 7.26 us
  waiting for transfers between devices: 48.7 us -> 0 us
  starting transfers between devices: 36.6 us -> 0 us
  matrix products: 35.5 us -> 0 us
  blocking collectives: 35.2 us -> 0 us
    pallas_call x0 -> x1, Pallas kernels: none -> 131 us  [body(): pl.pallas_call(functools.partial(kernel, nz, nyc, per_chunk), out_shape=(...]
    all_to_all x4 -> x0, waiting for transfers between devices: 48.7 us -> none  [the longest x1 25 us: expert_part(): lax.all_to_all(summed, EP, split_axis=0, concat_axis=0, tiled=True)]
    all_to_all x4 -> x0, starting transfers between devices: 36.6 us -> none  [the longest x1 13.8 us: expert_part(): lax.all_to_all(summed, EP, split_axis=0, concat_axis=0, tiled=True)]
    dot_general x28 -> x0, matrix products: 35.5 us -> none  [the longest x1 12.3 us: expert_part(): jnp.einsum('sif,fd->sid', (jax.nn.silu(gate_sum) * up_sum).astype(jnp.bfl...]
    all_gather x3 -> x0, blocking collectives: 35.2 us -> none  [gathered_once(): both, at, found = (lax.all_gather(jnp.concatenate(lines), axis), 0, {})]
    reduce_sum x13 -> x0, other arithmetic: 28.7 us -> none  [the longest x8 16.4 us: advance(): jnp.sum(block_queries[:, None] * block_keys[None, :] * decays, axis=-1)]
    dynamic_slice x24 -> x0, local copies, waits for them, and re-layouts: 16.3 us -> none  [gla_blocks(): lax.scan(advance, start_state, (blocked(query_single), blocked(key_float)...]
    another operation x13 -> x0, other arithmetic: 13.2 us -> none  [the longest x8 7.29 us: advance(): cumulative_decay = jnp.cumsum(gate_block, axis=0)]
  transfers between devices with their start and end apart: 4 -> 0, of which waited for: 3 -> 0; matrix products, arithmetic and copies ran while one was open for 37% -> 0% of each run, Pallas kernels for 0% -> 0%
where the time goes in v1:
time: 142 us; the launch traced here: 141 us
  Pallas kernels  131 us (92%)
  local copies, waits for them, and re-layouts  7.26 us (5%)
  other arithmetic  1.9 us (1%)
    pallas_call x1, Pallas kernels, body(): pl.pallas_call(functools.partial(kernel, nz, nyc, per_chunk), out_shape=(...  131 us
    unnamed x4, local copies, waits for them, and re-layouts  6.49 us

profile of v1, /device:TPU:1, one launch (start us, length us, event | category | flops | bytes accessed | tf_op | source)
XLA Modules:
  0.0 141.0 jit_solution(5709680500411950117)
XLA Ops:
  0.6 0.8 fusion.4
  1.4 1.5 %copy.19.chosen = f32[256,2]{1,0:T(8,128)} copy(f32[256,2]{0,1:T(2,128)} %param.28) | data formatting | bytes 4096 | tf_op args[12]
  2.9 1.5 %copy.18.routes = s32[256,2]{1,0:T(8,128)} copy(s32[256,2]{0,1:T(2,128)} %param.27) | data formatting | bytes 4096 | tf_op args[11]
  4.4 1.9 %fusion.3.log_decay = f32[512,128]{1,0:T(8,128)} fusion(bf16[512,128]{1,0:T(8,128)(2,1)} %param.19, f32[512]{0:T(512)S(1)} %bitcast.7, f32[512]{0:T(512)S(1)} %bitcast.6, f32[512]{0:T(512)} %param.21, f32[128]{0:T(128)} %param.20, pred[128]{0:T(512)(128)(4,1)S(1)} %iota_compare_fusion), kind=kLoop, calls=%fused_computation.4 | loop fusion | flops 851968 | bytes 400000 | tf_op jit(solution)/shard_map/add | solution.py:562
  6.3 131.2 %mixer_and_experts.1 = (bf16[128,2048]{1,0:T(8,128)(2,1)}, bf16[256,512]{1,0:T(8,128)(2,1)}) custom-call(s32[256,2]{1,0:T(8,128)} %copy.18.routes, s32[2,256]{1,0:T(2,128)} %bitcast.5, f32[256,2]{1,0:T(8,128)} %copy.19.chosen, bf16[256,2048]{1,0:T(8,128)(2,1)} %rows.1, f32[1,2048]{1,0:T(1,128)} %bitcast.4, bf16[512,128]{1,0:T(8,128)(2,1)} %queries.1, ...), custom_call_target="tpu_custom_call" | custom-call | tf_op jit(solution)/shard_map/mixer_and_experts/pallas_call | solution.py:567
  137.4 1.9 %copy.22 = bf16[128,2048]{1,0:T(8,128)(2,1)} copy(bf16[128,2048]{1,0:T(8,128)(2,1)} %get-tuple-element.6) | data formatting | bytes 1048576
  139.3 1.7 %copy.23 = bf16[256,512]{1,0:T(8,128)(2,1)} copy(bf16[256,512]{1,0:T(8,128)(2,1)} %get-tuple-element.7) | data formatting | bytes 524288
  (1 shorter events, 0.0 us)

commit v2 on v1

v2 whole, which is shorter than its diff:
```python
import functools

import jax
import jax.numpy as jnp
from jax import lax
from jax.experimental import pallas as pl
from jax.experimental.pallas import tpu as pltpu
from jax.sharding import Mesh
from jax.sharding import PartitionSpec as P

F32, BF16 = jnp.float32, jnp.bfloat16
MESH = pl.DeviceIdType.MESH
NX = 4
CAP = 16
BLOCK = 128
LEVELS = (64, 32, 16, 8, 4, 2, 1)
EPS = 1e-06
EP = ("z", "y", "c")
EP_TP = ("z", "y", "c", "tp")


def dot(a, b):
    return jnp.dot(a, b, preferred_element_type=F32)


def dot_nt(a, b):
    return lax.dot_general(a, b, (((1,), (1,)), ((), ())), preferred_element_type=F32)


def dot_tn(a, b):
    return lax.dot_general(a, b, (((0,), (0,)), ((), ())), preferred_element_type=F32)


def iota(shape, dim):
    return lax.broadcasted_iota(jnp.int32, shape, dim)


def one_where(mask):
    return jnp.where(mask, 1.0, 0.0)


CHUNKS = {
    1: ((0,),),
    2: ((0,), (1,)),
    8: ((6,), (2,), (5,), (3,), (4,), (7,), (1,), (0,)),
}
QUARTERS = {1: (2,), 2: (4, 1), 8: (1, 1, 1, 1, 1, 1, 1, 4)}
PLACE = (0, 2, 1, 3)
STEPS = (
    "ds1", "fy0", "ds6", "ds2", "fx0", "wr0", "fy1", "ds3", "ds5", "wy1", "fy6", "fx1", "ds4", "fy2", "wy2", "rl0",
    "fx6", "gla0", "ds7", "wy3", "fx2", "rl1", "fy5", "rl6", "fy3", "gla1", "gla2", "wz1", "fx5", "fx3", "ex0",
    "gla3", "rl5", "sy0", "rl2", "fy4", "rl3", "ap6", "fy7", "fx4", "ex3", "ex1", "ex2", "wz2", "wz3", "sz0", "rl4",
    "ap3", "gy6", "ap5", "ex5", "ex4", "gz6", "gy3", "ap2", "ex6", "gy5", "gz3", "ap4", "gz5", "ap7", "gy2", "ex7",
    "ap1", "cb6", "gz2", "gy4", "gy7", "ap0", "gz4", "wc0", "cb3", "gy1", "mx0", "gz7", "gy0", "cb2", "cb5", "gz1",
    "gz0", "me0", "cb4", "cb0", "cb7", "cb1",
)


def program_of(count):
    if count == 8:
        steps = STEPS
    else:
        order = sum(CHUNKS[count], ())
        quarters = QUARTERS[count]
        steps = [f"ds{d}" for d in order if d] + [f"fy{d}" for d in order]
        steps += ["wr0", "gla0", "gla1", "sy0", "wy1", "wy2", "wy3", "wz1", "wz2", "wz3", "wc0"]
        steps += [f"fx{d}" for d in order if quarters[d] < 4] + [f"rl{d}" for d in order if quarters[d] < 2]
        steps += ["sz0", "mx0"] + [f"ex{c}" for c in range(len(CHUNKS[count]))] + ["me0"]
        for name in ("ap", "gy", "gz", "cb"):
            steps += [f"{name}{d}" for d in order]
    return [(t.rstrip("0123456789"), int(t[len(t.rstrip("0123456789")) :])) for t in steps]


def kernel(
    nz,
    ny,
    nc,
    routes_t,
    chosen_t,
    gain,
    rate,
    position_factor,
    extra_t,
    head_gain,
    rows_hbm,
    queries_hbm,
    keys_hbm,
    values_hbm,
    forget_hbm,
    out_weight_hbm,
    gate_hbm,
    up_hbm,
    down_hbm,
    mix_out,
    moe_out,
    rows,
    queries,
    keys,
    values,
    forget,
    out_weight,
    input_sem,
    mix_held,
    moe_held,
    mixed,
    output_sem,
    gate_w,
    up_w,
    down_w,
    weight_sem,
    zsnd,
    zin,
    xq,
    part,
    pass_a,
    pass_b,
    from_left,
    from_right,
    result,
    yin,
    zret,
    zs,
    zr,
    ys,
    yr,
    xs,
    xr,
    ps,
    pr,
    y2s,
    y2r,
    z2s,
    z2r,
    sums,
    local_out,
    decayed_q,
    state,
    total,
    normed,
    sy,
    tz,
    sz,
    incoming,
    before,
    sys_,
    syr,
    szs,
    szr,
    normed_all,
    ms,
    mr,
    ws,
    wr,
):
    z, y, c, x = (lax.axis_index(a) for a in EP_TP)
    nyc = ny * nc
    yc = y * nc + c
    right, left, opposite = lax.rem(x + 1, NX), lax.rem(x + NX - 1, NX), lax.rem(x + 2, NX)

    def at_yc(index):
        return {"y": lax.div(index, nc), "c": lax.rem(index, nc)}

    order = sum(CHUNKS[nz], ())
    quarters = [QUARTERS[nz][d] for d in order]
    zrows = nyc * CAP
    half = zrows // 2
    quarter = rows.shape[1] // NX
    tokens = rows.shape[0]
    length = queries.shape[0]
    blocks = length // BLOCK

    def remote(src, dst, send, recv, device):
        return pltpu.make_async_remote_copy(
            src_ref=src, dst_ref=dst, send_sem=send, recv_sem=recv, device_id=device, device_id_type=MESH
        )

    def arrived(ref, sem):
        pltpu.make_async_copy(ref, ref, sem).wait()

    def times(value, unit):
        return pl.multiple_of(value * unit, unit)

    def columns(r):
        return pl.ds(PLACE[r] * quarter, quarter)

    def leading(k):
        return pl.ds(0, quarters[k] * quarter)

    barrier = pltpu.get_barrier_semaphore()
    pl.semaphore_signal(barrier, inc=1, device_id={"tp": right}, device_id_type=MESH)
    pl.semaphore_signal(barrier, inc=1, device_id={"tp": left}, device_id_type=MESH)

    pl.semaphore_signal(barrier, inc=1, device_id={"tp": opposite}, device_id_type=MESH)

    def greet_z(t, carry):
        pl.semaphore_signal(barrier, inc=1, device_id={"z": lax.rem(z + t, nz)}, device_id_type=MESH)
        return carry

    def greet_y(t, carry):
        pl.semaphore_signal(barrier, inc=1, device_id=at_yc(lax.rem(yc + t, nyc)), device_id_type=MESH)
        return carry

    lax.fori_loop(1, nz, greet_z, 0)
    lax.fori_loop(1, nyc, greet_y, 0)

    inputs = [
        pltpu.make_async_copy(a, b, input_sem.at[n])
        for n, (a, b) in enumerate(
            (
                (rows_hbm, rows),
                (forget_hbm, forget),
                (queries_hbm, queries),
                (keys_hbm, keys),
                (values_hbm, values),
                (out_weight_hbm, out_weight.at[0]),
            )
        )
    ]
    for load in inputs:
        load.start()
    loads = []
    for r in range(NX):
        back = times(lax.rem(x + NX - r, NX), quarter)
        ahead = times(lax.rem(x + r, NX), quarter)
        loads += [
            pltpu.make_async_copy(gate_hbm.at[0, pl.ds(back, quarter), :], gate_w.at[columns(r), :], weight_sem.at[0]),
            pltpu.make_async_copy(up_hbm.at[0, pl.ds(back, quarter), :], up_w.at[columns(r), :], weight_sem.at[1]),
            pltpu.make_async_copy(down_hbm.at[0, :, pl.ds(ahead, quarter)], down_w.at[:, columns(r)], weight_sem.at[2]),
        ]
    for load in loads:
        load.start()

    experts = nz * nyc
    first_t, second_t = routes_t[0:1, :], routes_t[1:2, :]
    marks = [one_where(iota((experts, tokens), 0) == e) for e in (first_t, second_t)]
    upper = one_where(iota((tokens, tokens), 0) < iota((tokens, tokens), 1)).astype(BF16)
    ranks = [dot(m.astype(BF16), upper) for m in marks]
    ranks[1] = ranks[1] + jnp.sum(marks[0], axis=1, keepdims=True)
    slots_t = [
        e.astype(F32) * CAP + jnp.sum(m * r, axis=0, keepdims=True)
        for e, m, r in zip((first_t, second_t), marks, ranks)
    ]

    inputs[0].wait()
    squares = rows[...].astype(F32)
    scale = lax.rsqrt(jnp.mean(squares * squares, axis=1, keepdims=True) + EPS)

    def moe_normed(r):
        here = pl.ds(times(lax.rem(x + NX - r, NX), quarter), quarter)
        return (rows[:, here].astype(F32) * scale * gain[:, here]).astype(BF16)

    own = moe_normed(0)

    pl.semaphore_wait(barrier, 3 + (nz - 1) + (nyc - 1))

    def dispatch(d):
        k = order.index(d)
        slot = (iota((zrows, tokens), 0) + lax.rem(z + d, nz) * zrows).astype(F32)
        chooser = one_where((slot == slots_t[0]) | (slot == slots_t[1])).astype(BF16)
        for r in (0, 2, 1, 3):
            if PLACE[r] < quarters[k]:
                zsnd[k, :, columns(r)] = dot(chooser, moe_normed(r) if r else own).astype(BF16)

    def send_z(k):
        target = {"z": lax.rem(z + order[k], nz)}
        remote(zsnd.at[k, :, leading(k)], zin.at[k, :, leading(k)], zs.at[quarters[k] // 2], zr.at[k], target).start()

    def forward_y(k):
        source = zin if order[k] else zsnd
        if order[k]:
            arrived(zin.at[k, :, leading(k)], zr.at[k])
        there = pl.ds(pl.multiple_of(k * zrows + yc * CAP, CAP), CAP)

        def send(t, carry):
            to = lax.rem(yc + t, nyc)
            remote(
                source.at[k, pl.ds(times(to, CAP), CAP), leading(k)],
                xq.at[there, leading(k)],
                ys.at[quarters[k] // 2],
                yr.at[k],
                at_yc(to),
            ).start()
            return carry

        lax.fori_loop(1, nyc, send, 0)
        xq[there, leading(k)] = source[k, pl.ds(times(yc, CAP), CAP), leading(k)]

    def forward_x(k):
        mine = xq.at[pl.ds(k * zrows, zrows), columns(0)]
        arrived(xq.at[pl.ds(k * zrows, zrows - CAP), leading(k)], yr.at[k])
        remote(mine, xq.at[pl.ds(k * zrows, zrows), columns(1)], xs.at[0], xr.at[0, k], {"tp": right}).start()
        remote(mine, xq.at[pl.ds(k * zrows, zrows), columns(3)], xs.at[1], xr.at[1, k], {"tp": left}).start()

    def relay(k):
        a, b = pl.ds(k * zrows, half), pl.ds(k * zrows + half, half)
        arrived(xq.at[pl.ds(k * zrows, zrows), columns(1)], xr.at[0, k])
        remote(xq.at[a, columns(1)], xq.at[a, columns(2)], xs.at[2], xr.at[2, k], {"tp": right}).start()
        arrived(xq.at[pl.ds(k * zrows, zrows), columns(3)], xr.at[1, k])
        remote(xq.at[b, columns(3)], xq.at[b, columns(2)], xs.at[3], xr.at[3, k], {"tp": left}).start()

    started = []

    def expert(c):
        first = order.index(CHUNKS[nz][c][0])
        members = range(first, first + len(CHUNKS[nz][c]))
        for k in members:
            if quarters[k] == 4:
                arrived(xq.at[pl.ds(k * zrows, zrows - CAP), :], yr.at[k])
            elif quarters[k] == 2:
                arrived(xq.at[pl.ds(k * zrows, zrows), columns(1)], xr.at[0, k])
                arrived(xq.at[pl.ds(k * zrows, zrows), columns(3)], xr.at[1, k])
            else:
                arrived(xq.at[pl.ds(k * zrows, half), columns(2)], xr.at[2, k])
                arrived(xq.at[pl.ds(k * zrows + half, half), columns(2)], xr.at[3, k])
        if not started:
            started.append(c)
            for n, weight in enumerate((gate_w, up_w, down_w)):
                arrived(weight, weight_sem.at[n])
        here = pl.ds(first * zrows, len(members) * zrows)
        gate = dot(xq[here, :], gate_w[...])
        up = dot(xq[here, :], up_w[...])
        hidden = (jax.nn.silu(gate) * up).astype(BF16)
        part[here, :] = dot(hidden, down_w[...]).astype(BF16)
        for k in members:
            a, b = pl.ds(k * zrows, half), pl.ds(k * zrows + half, half)
            remote(part.at[a, columns(2)], pass_a.at[k], ps.at[0], pr.at[0, k], {"tp": right}).start()
            remote(part.at[b, columns(2)], pass_b.at[k], ps.at[1], pr.at[1, k], {"tp": left}).start()

    def add_pass(k):
        here = pl.ds(k * zrows, zrows)
        a, b = pl.ds(k * zrows, half), pl.ds(k * zrows + half, half)
        arrived(pass_a.at[k], pr.at[0, k])
        part[a, columns(1)] = (part[a, columns(1)].astype(F32) + pass_a[k].astype(F32)).astype(BF16)
        remote(part.at[here, columns(1)], from_left.at[here], ps.at[2], pr.at[2, k], {"tp": right}).start()
        arrived(pass_b.at[k], pr.at[1, k])
        part[b, columns(3)] = (part[b, columns(3)].astype(F32) + pass_b[k].astype(F32)).astype(BF16)
        remote(part.at[here, columns(3)], from_right.at[here], ps.at[3], pr.at[3, k], {"tp": left}).start()

    def give_back_y(k):
        here = pl.ds(k * zrows, zrows)
        arrived(from_left.at[here], pr.at[2, k])
        arrived(from_right.at[here], pr.at[3, k])
        result[here, :] = (
            part[here, columns(0)].astype(F32) + from_left[here, :].astype(F32) + from_right[here, :].astype(F32)
        ).astype(BF16)

        def send(t, carry):
            to = lax.rem(yc + t, nyc)
            remote(
                result.at[pl.ds(pl.multiple_of(k * zrows + to * CAP, CAP), CAP), :],
                yin.at[k, pl.ds(times(yc, CAP), CAP), :],
                y2s,
                y2r.at[k],
                at_yc(to),
            ).start()
            return carry

        lax.fori_loop(1, nyc, send, 0)
        yin[k, pl.ds(times(yc, CAP), CAP), :] = result[pl.ds(pl.multiple_of(k * zrows + yc * CAP, CAP), CAP), :]

    def give_back_z(k):
        arrived(yin.at[k, pl.ds(0, zrows - CAP), :], y2r.at[k])
        if order[k]:
            to = lax.rem(z + nz - order[k], nz)
            remote(yin.at[k], zret.at[k], z2s, z2r.at[k], {"z": to}).start()

    combined = []

    def combine(k):
        base = lax.rem(z + order[k], nz) * zrows
        slot = (iota((zrows, tokens), 0) + base).astype(F32)
        weight = jnp.where(slot == slots_t[0], chosen_t[0:1, :], 0.0) + jnp.where(slot == slots_t[1], chosen_t[1:2, :], 0.0)
        high = weight.astype(BF16)
        low = (weight - high.astype(F32)).astype(BF16)
        if order[k]:
            arrived(zret.at[k], z2r.at[k])
        returned = zret[k] if order[k] else yin[k]
        fresh = dot_tn(high, returned) + dot_tn(low, returned)
        mixed[...] = mixed[...] + fresh if combined else fresh
        combined.append(k)

    def prepare_sums():
        i, j = iota((BLOCK, BLOCK), 0), iota((BLOCK, BLOCK), 1)
        for level, h in enumerate(LEVELS):
            edge = (i & ~(2 * h - 1)) + h
            after = (j >= edge) & (j <= i)
            ahead = (j > i) & (j < edge)
            m = one_where(after | ahead).astype(BF16)
            sums[pl.ds(level * BLOCK, BLOCK), pl.ds(0, BLOCK)] = m
            sums[pl.ds(level * BLOCK, BLOCK), pl.ds(BLOCK, BLOCK)] = m
        for level, m in ((len(LEVELS), j <= i), (len(LEVELS) + 1, j > i)):
            m = one_where(m).astype(BF16)
            sums[pl.ds(level * BLOCK, BLOCK), pl.ds(0, BLOCK)] = m
            sums[pl.ds(level * BLOCK, BLOCK), pl.ds(BLOCK, BLOCK)] = m

    first_head = iota((BLOCK, BLOCK), 1) < BLOCK // 2

    def by_head(value):
        return jnp.concatenate([jnp.where(first_head, value, 0.0), jnp.where(first_head, 0.0, value)], axis=0).astype(BF16)

    def gla_block(b):
        if b == 0:
            for load in inputs[1:5]:
                load.wait()
        r = pl.ds(b * BLOCK, BLOCK)
        factors = jnp.concatenate([position_factor[:, r], extra_t[:, r], jnp.zeros((5, BLOCK), F32)], axis=0).T
        f = forget[r, :].astype(F32)
        g = (jnp.minimum(f, 0.0) - jnp.log1p(jnp.exp(-jnp.abs(f)))) * rate[...] * factors[:, 0:1]
        g = g + jnp.where(first_head, factors[:, 1:2], factors[:, 2:3])
        high = g.astype(BF16)
        low = (g - high.astype(F32)).astype(BF16)
        e = jnp.exp(dot(sums[...], jnp.concatenate([high, low], axis=0)))
        q, k = queries[r, :].astype(F32), keys[r, :].astype(F32)
        i, j = iota((BLOCK, 2 * BLOCK), 0), iota((BLOCK, 2 * BLOCK), 1) & (BLOCK - 1)
        apart = i ^ j
        scores = None
        for level, h in enumerate(LEVELS):
            factor = e[level * BLOCK : (level + 1) * BLOCK]
            s = dot_nt((q * factor).astype(BF16), by_head(k * factor))
            scores = s if scores is None else jnp.where(apart < 2 * h, s, scores)
        scores = jnp.where(apart < 1, dot_nt(queries[r, :], by_head(k)), scores)
        scores = jnp.where(i >= j, scores, 0.0).astype(BF16)
        n = len(LEVELS)
        from_start = e[n * BLOCK : (n + 1) * BLOCK]
        to_end = e[(n + 1) * BLOCK : (n + 2) * BLOCK]
        qg = q * from_start
        outs = [
            dot(scores[:, h * BLOCK : (h + 1) * BLOCK], values[r, pl.ds(h * BLOCK, BLOCK)]) for h in range(2)
        ]
        if b:
            carried = dot_nt(by_head(qg), state[...].astype(BF16))
            outs = [o + carried[h * BLOCK : (h + 1) * BLOCK] for h, o in enumerate(outs)]
            decayed_q[r, :] = (qg * total[...]).astype(BF16)
        else:
            decayed_q[r, :] = qg.astype(BF16)
        for h in range(2):
            local_out[r, pl.ds(h * BLOCK, BLOCK)] = outs[h]
        grown = dot_tn(values[r, :], (k * to_end).astype(BF16))
        fresh = jnp.where(first_head, grown[0:BLOCK], grown[BLOCK : 2 * BLOCK])
        through = from_start[BLOCK - 1 : BLOCK, :]
        if b:
            state[...] = state[...] * through + fresh
            total[...] = total[...] * through
        else:
            state[...] = fresh
            total[...] = through

    def packed(s, d):
        high = d.astype(BF16).astype(F32)
        row = iota((16, BLOCK), 0)
        tail = jnp.where(row == 0, high, jnp.where(row == 1, d - high, 0.0))
        return s.astype(BF16), tail.astype(BF16)

    def opened(ref, at):
        tail = ref[at, pl.ds(BLOCK, 16), :].astype(F32)
        return ref[at, pl.ds(0, BLOCK), :].astype(F32), tail[0:1] + tail[1:2]

    def states_y():
        s, tail = packed(state[...], total[...])
        tz[1, pl.ds(0, BLOCK), :] = s
        tz[1, pl.ds(BLOCK, 16), :] = tail

        def send(t, carry):
            to = lax.rem(yc + t, nyc)
            remote(tz.at[1], sy.at[yc], sys_, syr, at_yc(to)).start()
            return carry

        lax.fori_loop(1, nyc, send, 0)
        sy[yc, pl.ds(0, BLOCK), :] = s
        sy[yc, pl.ds(BLOCK, 16), :] = tail

    def states_z():
        arrived(sy.at[pl.ds(0, nyc - 1)], syr)
        run_s, run_d = jnp.zeros((BLOCK, BLOCK), F32), jnp.ones((1, BLOCK), F32)
        before[pl.ds(0, BLOCK), :] = run_s
        before[pl.ds(BLOCK, 8), :] = jnp.broadcast_to(run_d, (8, BLOCK))
        for s in range(nyc):
            new_s, new_d = opened(sy, s)
            run_s, run_d = run_s * new_d + new_s, run_d * new_d

            @pl.when(s < yc)
            def _(run_s=run_s, run_d=run_d):
                before[pl.ds(0, BLOCK), :] = run_s
                before[pl.ds(BLOCK, 8), :] = jnp.broadcast_to(run_d, (8, BLOCK))

        s, tail = packed(run_s, run_d)
        tz[0, pl.ds(0, BLOCK), :] = s
        tz[0, pl.ds(BLOCK, 16), :] = tail
        for d in range(1, nz):

            @pl.when(z + d < nz)
            def _(d=d):
                remote(tz.at[0], sz.at[z], szs.at[d], szr.at[z], {"z": z + d}).start()

    def states_in():
        incoming[...] = jnp.zeros((BLOCK, BLOCK), F32)
        for s in range(nz - 1):

            @pl.when(s < z)
            def _(s=s):
                arrived(sz.at[s], szr.at[s])
                new_s, new_d = opened(sz, s)
                incoming[...] = incoming[...] * new_d + new_s

        incoming[...] = incoming[...] * before[pl.ds(BLOCK, 8), :][0:1] + before[pl.ds(0, BLOCK), :]

    mrows = length // NX
    width_of_group = 2 * BLOCK

    def mix():
        s = incoming[...].astype(BF16)
        for b in range(blocks):
            r = pl.ds(b * BLOCK, BLOCK)
            carried = dot_nt(by_head(decayed_q[r, :].astype(F32)), s)
            for h in range(2):
                c = pl.ds(h * BLOCK, BLOCK)
                o = local_out[r, c] + carried[h * BLOCK : (h + 1) * BLOCK]
                o = o * lax.rsqrt(jnp.mean(o * o, axis=1, keepdims=True) + EPS) * head_gain[h : h + 1, :]
                normed[r, c] = o.astype(BF16)
        normed_all[:, 0:width_of_group] = normed[pl.ds(times(x, mrows), mrows), :]
        for r, to in ((1, right), (2, opposite), (3, left)):
            remote(
                normed.at[pl.ds(times(to, mrows), mrows), :],
                normed_all.at[:, pl.ds(r * width_of_group, width_of_group)],
                ms,
                mr.at[r],
                {"tp": to},
            ).start()

    piece = out_weight.shape[1] // nyc
    phalf = piece // 2
    above, below = lax.rem(y + 1, ny), lax.rem(y + ny - 1, ny)

    def piece_of(which, start, size):
        return pl.ds(pl.multiple_of((c * ny + which) * piece + start, 16), size)

    def weights_x():
        inputs[5].wait()
        here = piece_of(y, 0, piece)
        remote(out_weight.at[0, here], out_weight.at[1, here], ws, wr.at[0], {"tp": right}).start()
        remote(out_weight.at[0, here], out_weight.at[3, here], ws, wr.at[1], {"tp": left}).start()

    def weights_x_relay():
        here, a, b = piece_of(y, 0, piece), piece_of(y, 0, phalf), piece_of(y, phalf, phalf)
        arrived(out_weight.at[1, here], wr.at[0])
        remote(out_weight.at[1, a], out_weight.at[2, a], ws, wr.at[2], {"tp": right}).start()
        arrived(out_weight.at[3, here], wr.at[1])
        remote(out_weight.at[3, b], out_weight.at[2, b], ws, wr.at[3], {"tp": left}).start()

    others = pl.ds(1, NX - 1)

    def weights_y(r):
        here, a, b = piece_of(y, 0, piece), piece_of(y, 0, phalf), piece_of(y, phalf, phalf)
        if r == 2:
            arrived(out_weight.at[2, a], wr.at[2])
            arrived(out_weight.at[2, b], wr.at[3])
        if ny > 1:
            mine = out_weight.at[r, here]
            remote(mine, mine, ws, wr.at[4 * r], {"y": above}).start()
            remote(mine, mine, ws, wr.at[4 * r + 1], {"y": below}).start()

    def weights_y_relay(r):
        if ny > 1:
            arrived(out_weight.at[r, piece_of(below, 0, piece)], wr.at[4 * r])
            a = out_weight.at[r, piece_of(below, 0, phalf)]
            remote(a, a, ws, wr.at[4 * r + 2], {"y": above}).start()
            arrived(out_weight.at[r, piece_of(above, 0, piece)], wr.at[4 * r + 1])
            b = out_weight.at[r, piece_of(above, phalf, phalf)]
            remote(b, b, ws, wr.at[4 * r + 3], {"y": below}).start()

    def column_of(which):
        return out_weight.at[others, pl.ds(times(which * ny, piece), ny * piece)]

    def weights_c():
        if ny > 1:
            far = lax.rem(y + 2, ny)
            for r in range(1, NX):
                arrived(out_weight.at[r, piece_of(far, 0, phalf)], wr.at[4 * r + 2])
                arrived(out_weight.at[r, piece_of(far, phalf, phalf)], wr.at[4 * r + 3])
        if nc > 1:
            remote(column_of(c), column_of(c), ws, wr.at[4 * NX], {"c": 1 - c}).start()

    def mix_end():
        if nc > 1:
            arrived(column_of(1 - c), wr.at[4 * NX])
        for r in range(1, NX):
            arrived(normed_all.at[:, pl.ds(r * width_of_group, width_of_group)], mr.at[r])
        full = out_weight[...].reshape(NX * width_of_group, out_weight.shape[2])
        mix_held[...] = dot(normed_all[...], full).astype(BF16)
        pltpu.make_async_copy(mix_held, mix_out, output_sem.at[0]).start()

    def at(work):
        return lambda d: work(order.index(d))

    def alone(*works):
        def run(index):
            for work in works:
                work()

        return run

    does = {
        "ds": at(send_z),
        "fy": at(forward_y),
        "fx": at(forward_x),
        "rl": at(relay),
        "ex": expert,
        "ap": at(add_pass),
        "gy": at(give_back_y),
        "gz": at(give_back_z),
        "cb": at(combine),
        "gla": gla_block,
        "sy": alone(states_y),
        "sz": alone(states_z),
        "mx": alone(states_in, mix),
        "me": alone(mix_end),
        "wr": alone(weights_x_relay),
        "wy": weights_y,
        "wz": weights_y_relay,
        "wc": alone(weights_c),
    }
    weights_x()
    for d in sorted(order, key=lambda d: min(d, nz - d)):
        dispatch(d)
    for name, index in program_of(nz):
        if (name, index) == ("gla", 0):
            prepare_sums()
        does[name](index)
    moe_held[...] = mixed[...].astype(BF16)
    pltpu.make_async_copy(moe_held, moe_out, output_sem.at[1]).start()

    for q in sorted(set(quarters)):
        across = pl.ds(0, q * quarter)
        forwarded = quarters.count(q)
        sent = forwarded - (quarters[order.index(0)] == q)
        arrived(xq.at[pl.ds(0, forwarded * (zrows - CAP)), across], ys.at[q // 2])
        if sent:
            arrived(xq.at[pl.ds(0, sent * zrows), across], zs.at[q // 2])
    gathered, relayed = sum(q < 4 for q in quarters), sum(q < 2 for q in quarters)
    for side in range(2):
        if gathered:
            arrived(xq.at[pl.ds(0, gathered * zrows), columns(0)], xs.at[side])
        if relayed:
            arrived(xq.at[pl.ds(0, relayed * half), columns(0)], xs.at[2 + side])
        arrived(xq.at[pl.ds(0, nz * half), columns(0)], ps.at[side])
        arrived(xq.at[pl.ds(0, nz * zrows), columns(0)], ps.at[2 + side])
    arrived(xq.at[pl.ds(0, nz * (zrows - CAP)), columns(0)], y2s)
    if nz > 1:
        arrived(xq.at[pl.ds(0, (nz - 1) * zrows), columns(0)], z2s)
    arrived(sy.at[pl.ds(0, nyc - 1)], sys_)
    for d in range(1, nz):

        @pl.when(z + d < nz)
        def _(d=d):
            arrived(tz.at[0], szs.at[d])

    arrived(normed_all.at[:, pl.ds(0, (NX - 1) * width_of_group)], ms)
    sent = 2 * (piece + phalf) * (NX if ny > 1 else 1) + ((NX - 1) * ny * piece if nc > 1 else 0)
    arrived(out_weight.at[pl.ds(0, sent // out_weight.shape[1])], ws)
    pltpu.make_async_copy(mix_held, mix_out, output_sem.at[0]).wait()
    pltpu.make_async_copy(moe_held, moe_out, output_sem.at[1]).wait()


def body(
    nz,
    ny,
    nc,
    queries,
    key_rows,
    value_rows,
    forget_gate_input,
    channel_decay_rate,
    position_decay_factor,
    extra_log_decay,
    head_norm_gain,
    output_projection_weight,
    expert_input_rows,
    expert_norm_gain,
    routes,
    chosen_expert_weights,
    expert_gate_weight,
    expert_up_weight,
    expert_down_weight,
):
    length, channels = queries.shape
    tokens, width = expert_input_rows.shape
    hidden = expert_gate_weight.shape[2]
    quarter = width // NX
    nyc = ny * nc
    zrows = nyc * CAP
    dma, vmem = pltpu.SemaphoreType.DMA, pltpu.VMEM
    mrows = length // NX
    outs = pl.pallas_call(
        functools.partial(kernel, nz, ny, nc),
        out_shape=(
            jax.ShapeDtypeStruct((mrows, width), BF16),
            jax.ShapeDtypeStruct((tokens, quarter), BF16),
        ),
        in_specs=[pl.BlockSpec(memory_space=vmem)] * 7 + [pl.BlockSpec(memory_space=pl.ANY)] * 9,
        out_specs=(pl.BlockSpec(memory_space=pl.ANY), pl.BlockSpec(memory_space=pl.ANY)),
        scratch_shapes=[
            vmem((tokens, width), BF16),
            vmem((length, channels), BF16),
            vmem((length, channels), BF16),
            vmem((length, value_rows.shape[1]), BF16),
            vmem((length, channels), BF16),
            vmem((NX, *output_projection_weight.shape), BF16),
            dma((6,)),
            vmem((mrows, width), BF16),
            vmem((tokens, quarter), BF16),
            vmem((tokens, quarter), F32),
            dma((2,)),
            vmem((width, hidden), BF16),
            vmem((width, hidden), BF16),
            vmem((hidden, width), BF16),
            dma((3,)),
            vmem((nz, zrows, width), BF16),
            vmem((nz, zrows, width), BF16),
            vmem((nz * zrows, width), BF16),
            vmem((nz * zrows, width), BF16),
            vmem((nz, zrows // 2, quarter), BF16),
            vmem((nz, zrows // 2, quarter), BF16),
            vmem((nz * zrows, quarter), BF16),
            vmem((nz * zrows, quarter), BF16),
            vmem((nz * zrows, quarter), BF16),
            vmem((nz, zrows, quarter), BF16),
            vmem((nz, zrows, quarter), BF16),
            dma((3,)),
            dma((nz,)),
            dma((3,)),
            dma((nz,)),
            dma((4,)),
            dma((4, nz)),
            dma((4,)),
            dma((4, nz)),
            dma(()),
            dma((nz,)),
            dma(()),
            dma((nz,)),
            vmem(((len(LEVELS) + 2) * BLOCK, 2 * BLOCK), BF16),
            vmem((length, 2 * BLOCK), F32),
            vmem((length, BLOCK), BF16),
            vmem((BLOCK, BLOCK), F32),
            vmem((1, BLOCK), F32),
            vmem((length, 2 * BLOCK), BF16),
            vmem((nyc, BLOCK + 16, BLOCK), BF16),
            vmem((2, BLOCK + 16, BLOCK), BF16),
            vmem((nz, BLOCK + 16, BLOCK), BF16),
            vmem((BLOCK, BLOCK), F32),
            vmem((BLOCK + 8, BLOCK), F32),
            dma(()),
            dma(()),
            dma((nz,)),
            dma((nz,)),
            vmem((mrows, NX * value_rows.shape[1]), BF16),
            dma(()),
            dma((NX,)),
            dma(()),
            dma((4 * NX + 1,)),
        ],
        compiler_params=pltpu.CompilerParams(
            collective_id=0, has_side_effects=True, vmem_limit_bytes=60 * 1024 * 1024
        ),
        name="mixer_and_experts",
    )(
        routes.T,
        chosen_expert_weights.T,
        expert_norm_gain[None, :],
        channel_decay_rate[None, :],
        position_decay_factor[None, :],
        extra_log_decay.T,
        head_norm_gain,
        expert_input_rows,
        queries,
        key_rows,
        value_rows,
        forget_gate_input,
        output_projection_weight,
        expert_gate_weight,
        expert_up_weight,
        expert_down_weight,
    )
    return pl.pallas_call(
        handed_over,
        out_shape=tuple(jax.ShapeDtypeStruct(o.shape, o.dtype) for o in outs),
        in_specs=[pl.BlockSpec(memory_space=vmem)] * 2,
        out_specs=(pl.BlockSpec(memory_space=vmem),) * 2,
        name="handed_over",
    )(*outs)


def handed_over(mix_in, moe_in, mix_out, moe_out):
    mix_out[...] = mix_in[...]
    moe_out[...] = moe_in[...]


def mapped(mesh, nz, ny, nc):
    finer = Mesh(mesh.devices.reshape(nz, ny, nc, NX), EP_TP)
    return jax.shard_map(
        functools.partial(body, nz, ny, nc),
        mesh=finer,
        in_specs=(
            P(EP, "tp"),
            P(EP, "tp"),
            P(EP, "tp"),
            P(EP, "tp"),
            P("tp"),
            P(EP),
            P(EP, "tp"),
            P("tp", None),
            P("tp", None),
            P(EP, None),
            P(),
            P(EP, None),
            P(EP, None),
            P(EP, None, "tp"),
            P(EP, None, "tp"),
            P(EP, "tp", None),
        ),
        out_specs=(P(EP_TP, None), P(EP, "tp")),
        check_vma=False,
    )


def solution(mesh):
    return mapped(mesh, 8, 4, 2)
```

time: 142 us -> 101 us (0.71)
  Pallas kernels: 131 us -> 100 us
  local copies, waits for them, and re-layouts: 7.26 us -> 0 us
  other arithmetic: 1.9 us -> 0 us
    pallas_call x1 -> x2, Pallas kernels: 131 us -> 100 us  [the longest x1 98.2 us: body(): pl.pallas_call(functools.partial(kernel, nz, ny, nc), out_shape=(jax.Shap...]
    unnamed x4 -> x0, local copies, waits for them, and re-layouts: 6.49 us -> none
    add x1 -> x0, other arithmetic: 1.89 us -> none  [body(): jax.nn.log_sigmoid(forget_gate_input.astype(F32))]
where the time goes in v2:
time: 101 us
  Pallas kernels  100 us (99%)
    pallas_call x1, Pallas kernels, body(): pl.pallas_call(functools.partial(kernel, nz, ny, nc), out_shape=(jax.Shap...  98.2 us

profile of v2, /device:TPU:1, one launch (start us, length us, event | category | flops | bytes accessed | tf_op | source)
XLA Modules:
  0.0 100.9 jit_solution(16966931437258111630)
XLA Ops:
  0.6 98.2 %mixer_and_experts.1 = (bf16[128,2048]{1,0:T(8,128)(2,1)}, bf16[256,512]{1,0:T(8,128)(2,1)}) custom-call(s32[2,256]{1,0:T(2,128)} %bitcast.8, f32[2,256]{1,0:T(2,128)} %bitcast.9, f32[1,2048]{1,0:T(1,128)} %bitcast.6, f32[1,128]{1,0:T(1,128)} %bitcast.11, f32[1,512]{1,0:T(1,128)} %bitcast.10, f32[2,512]{1,0:T(2,128)} %bitcast.7, f32[2,128]{1,0:T(2,128)} %head_gain.1, ...), custom_call_target="tpu_custom_call" | custom-call | tf_op jit(solution)/shard_map/mixer_and_experts/pallas_call | solution.py:693
  98.8 2.0 %handed_over.1 = (bf16[128,2048]{1,0:T(8,128)(2,1)}, bf16[256,512]{1,0:T(8,128)(2,1)}) custom-call(bf16[128,2048]{1,0:T(8,128)(2,1)} %get-tuple-element.4.mix_in, bf16[256,512]{1,0:T(8,128)(2,1)} %get-tuple-element.5.moe_in), custom_call_target="tpu_custom_call" | custom-call | tf_op jit(solution)/shard_map/handed_over/pallas_call | solution.py:783

commit v3 on v2

--- a/solution.py
+++ b/solution.py
@@ -75,13 +75,13 @@
     nz,
     ny,
     nc,
-    routes_t,
-    chosen_t,
-    gain,
-    rate,
-    position_factor,
-    extra_t,
-    head_gain,
+    routes_hbm,
+    chosen_hbm,
+    gain_hbm,
+    rate_hbm,
+    position_hbm,
+    extra_hbm,
+    head_gain_hbm,
     rows_hbm,
     queries_hbm,
     keys_hbm,
@@ -93,12 +93,20 @@
     down_hbm,
     mix_out,
     moe_out,
+    routes_t,
+    chosen_t,
+    gain,
+    rate,
+    position_factor,
+    extra_t,
+    head_gain,
     rows,
     queries,
     keys,
     values,
     forget,
     out_weight,
+    small_sem,
     input_sem,
     mix_held,
     moe_held,
@@ -203,6 +211,20 @@
     lax.fori_loop(1, nz, greet_z, 0)
     lax.fori_loop(1, nyc, greet_y, 0)
 
+    small = [
+        pltpu.make_async_copy(a, b, small_sem.at[n])
+        for n, (a, b) in enumerate(
+            (
+                (routes_hbm, routes_t),
+                (gain_hbm, gain),
+                (chosen_hbm, chosen_t),
+                (rate_hbm, rate),
+                (position_hbm, position_factor),
+                (extra_hbm, extra_t),
+                (head_gain_hbm, head_gain),
+            )
+        )
+    ]
     inputs = [
         pltpu.make_async_copy(a, b, input_sem.at[n])
         for n, (a, b) in enumerate(
@@ -216,7 +238,7 @@
             )
         )
     ]
-    for load in inputs:
+    for load in small[:1] + inputs[:1] + small[1:] + inputs[1:]:
         load.start()
     loads = []
     for r in range(NX):
@@ -230,6 +252,7 @@
     for load in loads:
         load.start()
 
+    small[0].wait()
     experts = nz * nyc
     first_t, second_t = routes_t[0:1, :], routes_t[1:2, :]
     marks = [one_where(iota((experts, tokens), 0) == e) for e in (first_t, second_t)]
@@ -241,6 +264,7 @@
         for e, m, r in zip((first_t, second_t), marks, ranks)
     ]
 
+    small[1].wait()
     inputs[0].wait()
     squares = rows[...].astype(F32)
     scale = lax.rsqrt(jnp.mean(squares * squares, axis=1, keepdims=True) + EPS)
@@ -250,8 +274,6 @@
         return (rows[:, here].astype(F32) * scale * gain[:, here]).astype(BF16)
 
     own = moe_normed(0)
-
-    pl.semaphore_wait(barrier, 3 + (nz - 1) + (nyc - 1))
 
     def dispatch(d):
         k = order.index(d)
@@ -400,7 +422,7 @@
 
     def gla_block(b):
         if b == 0:
-            for load in inputs[1:5]:
+            for load in small[2:] + inputs[1:5]:
                 load.wait()
         r = pl.ds(b * BLOCK, BLOCK)
         factors = jnp.concatenate([position_factor[:, r], extra_t[:, r], jnp.zeros((5, BLOCK), F32)], axis=0).T
@@ -619,12 +641,12 @@
         "wz": weights_y_relay,
         "wc": alone(weights_c),
     }
-    weights_x()
     for d in sorted(order, key=lambda d: min(d, nz - d)):
         dispatch(d)
+    prepare_sums()
+    pl.semaphore_wait(barrier, 3 + (nz - 1) + (nyc - 1))
+    weights_x()
     for name, index in program_of(nz):
-        if (name, index) == ("gla", 0):
-            prepare_sums()
         does[name](index)
     moe_held[...] = mixed[...].astype(BF16)
     pltpu.make_async_copy(moe_held, moe_out, output_sem.at[1]).start()
@@ -696,15 +718,23 @@
             jax.ShapeDtypeStruct((mrows, width), BF16),
             jax.ShapeDtypeStruct((tokens, quarter), BF16),
         ),
-        in_specs=[pl.BlockSpec(memory_space=vmem)] * 7 + [pl.BlockSpec(memory_space=pl.ANY)] * 9,
+        in_specs=[pl.BlockSpec(memory_space=pl.ANY)] * 16,
         out_specs=(pl.BlockSpec(memory_space=pl.ANY), pl.BlockSpec(memory_space=pl.ANY)),
         scratch_shapes=[
+            vmem((routes.shape[1], tokens), routes.dtype),
+            vmem((routes.shape[1], tokens), F32),
+            vmem((1, width), F32),
+            vmem((1, channels), F32),
+            vmem((1, length), F32),
+            vmem((extra_log_decay.shape[1], length), F32),
+            vmem(head_norm_gain.shape, F32),
             vmem((tokens, width), BF16),
             vmem((length, channels), BF16),
             vmem((length, channels), BF16),
             vmem((length, value_rows.shape[1]), BF16),
             vmem((length, channels), BF16),
             vmem((NX, *output_projection_weight.shape), BF16),
+            dma((7,)),
             dma((6,)),
             vmem((mrows, width), BF16),
             vmem((tokens, quarter), BF16),

time: 101 us -> 100 us (0.990)
    pallas_call x1, Pallas kernels: 98.2 us -> 96.9 us  [body(): pl.pallas_call(functools.partial(kernel, nz, ny, nc), out_shape=(jax.Shap...]
where the time goes in v3:
time: 100 us; the launch traced here: 99.6 us
  Pallas kernels  99 us (99%)
    pallas_call x1, Pallas kernels, body(): pl.pallas_call(functools.partial(kernel, nz, ny, nc), out_shape=(jax.Shap...  96.9 us
    pallas_call x1, Pallas kernels, body(): pl.pallas_call(handed_over, out_shape=tuple((jax.ShapeDtypeStruct(o.shape...  2.02 us

profile of v3, /device:TPU:1, one launch (start us, length us, event | category | flops | bytes accessed | tf_op | source)
XLA Modules:
  0.0 99.6 jit_solution(13209672221554519498)
XLA Ops:
  0.6 96.9 %mixer_and_experts.1 = (bf16[128,2048]{1,0:T(8,128)(2,1)}, bf16[256,512]{1,0:T(8,128)(2,1)}) custom-call(s32[2,256]{1,0:T(2,128)} %bitcast.8, f32[2,256]{1,0:T(2,128)} %bitcast.9, f32[1,2048]{1,0:T(1,128)} %bitcast.6, f32[1,128]{1,0:T(1,128)} %bitcast.11, f32[1,512]{1,0:T(1,128)} %bitcast.10, f32[2,512]{1,0:T(2,128)} %bitcast.7, f32[2,128]{1,0:T(2,128)} %head_gain_hbm.1, ...), custom_call_target="tpu_custom_call" | custom-call | tf_op jit(solution)/shard_map/mixer_and_experts/pallas_call | solution.py:715
  97.6 2.0 %handed_over.1 = (bf16[128,2048]{1,0:T(8,128)(2,1)}, bf16[256,512]{1,0:T(8,128)(2,1)}) custom-call(bf16[128,2048]{1,0:T(8,128)(2,1)} %get-tuple-element.4.mix_in, bf16[256,512]{1,0:T(8,128)(2,1)} %get-tuple-element.5.moe_in), custom_call_target="tpu_custom_call" | custom-call | tf_op jit(solution)/shard_map/handed_over/pallas_call | solution.py:813
